TPU v7x, 512 devices: a whole 4x4x16 slice. The times are simulated.
512 devices in a mesh: sp: 16 (over z), dp: 32 (over y, x, core).
Axes of the slice: x: 4, y: 4, z: 16, core: 2. Of those that a mesh axis runs over, the one named last changes fastest.
Arguments:
- queries: bfloat16 [32, 2048, 1024], P('dp', 'sp'), may hold values from -6 to 6
- key_rows: bfloat16 [32, 2048, 1024], P('dp', 'sp'), may hold values from -6 to 6
- value_rows: bfloat16 [32, 2048, 1024], P('dp', 'sp'), may hold values from -6 to 6
- break_offset: bfloat16 [32, 2048, 16], P('dp', 'sp'), may hold values from 1.5 to 15
- hidden_in: bfloat16 [32, 2048, 2048], P('dp', 'sp'), may hold values from -6 to 6
- gate_weight: bfloat16 [2048, 1024], P('dp', 'sp'), may hold values from -0.125 to 0.125
- out_weight: bfloat16 [1024, 2048], P('sp', 'dp'), may hold values from -0.1875 to 0.1875
Outputs:
- mixed: bfloat16 [32, 2048, 2048], P('dp', 'sp')
All inputs are finite; a program needn't handle non-finite values.
Results may differ from a plain program's by a relative error of at most 0.0063.
Values may be sent and summed in bfloat16 or wider, within the bound.
No kernel may reach another device: no remote copies, remote signals or barrier semaphores. Data moves between devices by JAX's collectives and lax.ppermute only.
A program may use at most 64 MiB of HBM per device.

v0:
```python
import jax
import jax.numpy as jnp
from jax import lax
from jax.sharding import PartitionSpec as P

eps_norm = 1e-05


def turned_gather(arrays, axis, dims):
    turned = [jnp.moveaxis(a, dim, 0) for a, dim in zip(arrays, dims)]
    widths = [t[0].size for t in turned]
    both = jnp.concatenate([t.reshape(-1, w) for t, w in zip(turned, widths)], axis=1)
    out = lax.all_gather(both, axis, axis=0, tiled=True)
    blocks = jnp.split(out, [sum(widths[:k]) for k in range(1, len(widths))], axis=1)
    return tuple(
        (
            jnp.moveaxis(b.reshape(-1, *t.shape[1:]), 0, dim)
            for b, t, dim in zip(blocks, turned, dims)
        )
    )


def stick_blocks(head_queries, head_keys, head_values, head_offsets):
    groups, length, head_size = head_queries.shape
    block_rows = min(512, length)
    block_count = length // block_rows
    score_scale = head_size ** (-0.5)
    query_blocks = head_queries.reshape(groups, block_count, block_rows, head_size)

    def one_block(block_index):
        query_block = lax.dynamic_index_in_dim(query_blocks, block_index, 1, keepdims=False)
        query_pos = block_index * block_rows + jnp.arange(block_rows, dtype=jnp.int32)

        def key_step(step_turn, carry):
            running, carried = carry
            key_first = (block_index - step_turn) * block_rows
            key_block = lax.dynamic_slice_in_dim(head_keys, key_first, block_rows, 1)
            value_block = lax.dynamic_slice_in_dim(head_values, key_first, block_rows, 1)
            offset_block = lax.dynamic_slice_in_dim(head_offsets, key_first, block_rows, 1)
            scores = jnp.einsum(
                "gqd,gkd->gqk", query_block, key_block, preferred_element_type=jnp.float32
            )
            scores = scores * score_scale - offset_block[:, None, :]
            key_pos = key_first + jnp.arange(block_rows, dtype=jnp.int32)
            earlier = key_pos[None, :] < query_pos[:, None]
            keep_log = jnp.where(earlier, jax.nn.log_sigmoid(-scores), 0.0)
            later_sum = lax.cumsum(keep_log, axis=2, reverse=True) - keep_log + carried
            weights = jnp.where(
                earlier, jnp.exp(jax.nn.log_sigmoid(scores) + later_sum), 0.0
            ).astype(jnp.bfloat16)
            running = running + jnp.einsum(
                "gqk,gkd->gqd", weights, value_block, preferred_element_type=jnp.float32
            )
            carried = carried + jnp.sum(keep_log, axis=2, keepdims=True)
            return (running, carried)

        start_carry = (
            jnp.zeros((groups, block_rows, head_size), jnp.float32),
            jnp.zeros((groups, block_rows, 1), jnp.float32),
        )
        running, carried = lax.fori_loop(0, block_index + 1, key_step, start_carry)
        return running

    outputs = lax.map(one_block, jnp.arange(block_count, dtype=jnp.int32))
    return outputs.transpose(1, 0, 2, 3).reshape(groups, length, head_size)


def attend(pieces):
    head_queries, head_keys, head_values, head_offsets = pieces
    item_count, length, feature_count = head_queries.shape
    heads_dev = head_offsets.shape[2]
    head_size = feature_count // heads_dev

    def split_heads(array):
        return (
            array.reshape(item_count, length, heads_dev, head_size)
            .transpose(0, 2, 1, 3)
            .reshape(item_count * heads_dev, length, head_size)
        )

    offsets = (
        head_offsets.transpose(0, 2, 1).reshape(item_count * heads_dev, length).astype(jnp.float32)
    )
    heads_out = stick_blocks(
        split_heads(head_queries), split_heads(head_keys), split_heads(head_values), offsets
    )
    mean_sq = jnp.mean(heads_out * heads_out, axis=2, keepdims=True)
    normed = (heads_out * lax.rsqrt(mean_sq + eps_norm)).astype(jnp.bfloat16)
    return (
        normed.reshape(item_count, heads_dev, length, head_size)
        .transpose(0, 2, 1, 3)
        .reshape(item_count, length, feature_count)
    )


def shards(queries, key_rows, value_rows, break_offset, hidden_in, gate_weight, out_weight):
    tokens = hidden_in[0]
    gate_rows, out_cols = turned_gather((gate_weight, out_weight), "sp", (1, 0))
    gate_pre = jnp.dot(
        tokens,
        lax.all_gather(gate_rows, "dp", axis=0, tiled=True),
        preferred_element_type=jnp.float32,
    )
    gate_act = jax.nn.silu(gate_pre)
    normed = attend(
        (
            lax.all_to_all(queries, "sp", split_axis=2, concat_axis=1, tiled=True),
            lax.all_to_all(key_rows, "sp", split_axis=2, concat_axis=1, tiled=True),
            lax.all_to_all(value_rows, "sp", split_axis=2, concat_axis=1, tiled=True),
            lax.all_to_all(break_offset, "sp", split_axis=2, concat_axis=1, tiled=True),
        )
    )
    returned = lax.all_to_all(normed, "sp", split_axis=1, concat_axis=2, tiled=True)
    gated_rows = (returned[0].astype(jnp.float32) * gate_act).astype(jnp.bfloat16)
    mixed_rows = jnp.dot(
        gated_rows,
        lax.all_gather(out_cols, "dp", axis=1, tiled=True),
        preferred_element_type=jnp.float32,
    )
    return mixed_rows.astype(jnp.bfloat16)[None]


def solution(mesh):
    return jax.shard_map(
        shards,
        mesh=mesh,
        in_specs=(
            P("dp", "sp", None),
            P("dp", "sp", None),
            P("dp", "sp", None),
            P("dp", "sp", None),
            P("dp", "sp", None),
            P("dp", "sp"),
            P("sp", "dp"),
        ),
        out_specs=P("dp", "sp", None),
        check_vma=False,
    )
```

profile of v0, /device:TPU:54, one launch (start us, length us, event | category | flops | bytes accessed | tf_op | source)
XLA Modules:
  0.0 296.1 jit_solution(12190595315451277451)
XLA Ops:
  8.2 34.7 %all_gather.9 = bf16[1024,128]{1,0:T(8,128)(2,1)S(1)} all-gather(bf16[64,128]{1,0:T(8,128)(2,1)S(1)} %pad_maximum_fusion), channel_id=1, replica_groups=mesh['sp'=16,'dp'=32] {'sp'}, dimensions={0}, use_global_device_ids=true | all-gather | bytes 278528 | tf_op jit(solution)/shard_map/all_gather | solution.py:13
  45.1 8.9 %all-to-all-start.2 = ((bf16[1,128,16]{1,0,2:T(2,128)(2,1)}), bf16[1,128,16]{1,0,2:T(2,128)(2,1)S(1)}, u32[]{:S(2)}, u32[]{:S(2)}) async-start(bf16[1,128,16]{1,0,2:T(2,128)(2,1)} %copy.78), calls=%async_computation.2 | async-start | bytes 16384 | tf_op jit(solution)/shard_map/all_to_all | solution.py:110
  55.9 2.3 reduce.6
  58.9 6.1 %all-to-all-done.2 = bf16[1,128,16]{1,0,2:T(2,128)(2,1)S(1)} async-done(((bf16[1,128,16]{1,0,2:T(2,128)(2,1)}), bf16[1,128,16]{1,0,2:T(2,128)(2,1)S(1)}, u32[]{:S(2)}, u32[]{:S(2)}) %all-to-all-start.2) | async-done | bytes 4128 | tf_op jit(solution)/shard_map/all_to_all | solution.py:110
  65.1 5.9 %all-to-all-start.3 = ((bf16[16,2,4096]{2,1,0:T(2,128)(2,1)}), bf16[16,2,4096]{2,1,0:T(2,128)(2,1)S(1)}, u32[]{:S(2)}, u32[]{:S(2)}) async-start(bf16[16,2,4096]{2,1,0:T(2,128)(2,1)} %reshape.172), calls=%async_computation.3 | async-start | bytes 524288 | tf_op jit(solution)/shard_map/all_to_all | solution.py:109
  71.4 2.3 reduce.4
  74.5 11.4 %all-to-all-done.3 = bf16[16,2,4096]{2,1,0:T(2,128)(2,1)S(1)} async-done(((bf16[16,2,4096]{2,1,0:T(2,128)(2,1)}), bf16[16,2,4096]{2,1,0:T(2,128)(2,1)S(1)}, u32[]{:S(2)}, u32[]{:S(2)}) %all-to-all-start.3) | async-done | bytes 262176 | tf_op jit(solution)/shard_map/all_to_all | solution.py:109
  85.8 5.1 %all-to-all-start = ((bf16[16,2,4096]{2,1,0:T(2,128)(2,1)}), bf16[16,2,4096]{2,1,0:T(2,128)(2,1)S(1)}, u32[]{:S(2)}, u32[]{:S(2)}) async-start(bf16[16,2,4096]{2,1,0:T(2,128)(2,1)} %reshape.168), calls=%async_computation | async-start | bytes 524288 | tf_op jit(solution)/shard_map/all_to_all | solution.py:107
  91.3 2.3 reduce.5
  94.4 11.2 %all-to-all-done = bf16[16,2,4096]{2,1,0:T(2,128)(2,1)S(1)} async-done(((bf16[16,2,4096]{2,1,0:T(2,128)(2,1)}), bf16[16,2,4096]{2,1,0:T(2,128)(2,1)S(1)}, u32[]{:S(2)}, u32[]{:S(2)}) %all-to-all-start) | async-done | bytes 262176 | tf_op jit(solution)/shard_map/all_to_all | solution.py:107
  105.7 5.2 %all-to-all-start.1 = ((bf16[16,2,4096]{2,1,0:T(2,128)(2,1)}), bf16[16,2,4096]{2,1,0:T(2,128)(2,1)S(1)}, u32[]{:S(2)}, u32[]{:S(2)}) async-start(bf16[16,2,4096]{2,1,0:T(2,128)(2,1)} %reshape.170), calls=%async_computation.1 | async-start | bytes 524288 | tf_op jit(solution)/shard_map/all_to_all | solution.py:108
  114.0 11.4 %all-to-all-done.1 = bf16[16,2,4096]{2,1,0:T(2,128)(2,1)S(1)} async-done(((bf16[16,2,4096]{2,1,0:T(2,128)(2,1)}), bf16[16,2,4096]{2,1,0:T(2,128)(2,1)S(1)}, u32[]{:S(2)}, u32[]{:S(2)}) %all-to-all-start.1) | async-done | bytes 262176 | tf_op jit(solution)/shard_map/all_to_all | solution.py:108
  126.8 117.7 %while.24 = (s32[]{:T(128)}, f32[4,1,512,64]{2,3,1,0:T(8,128)}, s32[4]{0:T(128)S(1)}, bf16[1,4,512,64]{3,2,1,0:T(8,128)(2,1)}, bf16[1,2048,64]{2,1,0:T(8,128)(2,...) while((s32[]{:T(128)}, f32[4,1,512,64]{2,3,1,0:T(8,128)}, ...), condition=%wide.region_6.7_spmd, body=%wide.region_0.6_spmd.sunk | while | flops 109617680 | bytes 10642510 | solution.py:64
  131.5 9.6 %while.25 = (s32[]{:T(128)}, f32[1,512,64]{1,2,0:T(8,128)S(1)}, f32[1,512,1]{1,2,0:T(1,128)S(1)}, s32[]{:T(128)}, s32[]{:T(128)}, /*index=5*/bf16[1,2048,64]{2,1...) while((s32[]{:T(128)}, f32[1,512,64]{1,2,0:T(8,128)S(1)}, ...), condition=%wide.region_5.5_spmd.clone, body=%wide.region_1.4_spmd.clone.sunk | while | flops 109617672 | bytes 10115295 | solution.py:61
  132.1 1.9 fusion.42
  134.0 4.8 %fusion.43 = f32[1,512,4,128]{1,2,3,0:T(4,128)S(1)} fusion(f32[1,512,4,128]{1,3,2,0:T(8,128)S(1)} %bitcast.136), kind=kOutput, calls=%fused_computation.18.clone.1 | output fusion | flops 33292288 | bytes 2097152 | tf_op jit(solution)/shard_map/reduce-window
  139.2 1.6 fusion.44
  146.5 19.2 %while.25 = (s32[]{:T(128)}, f32[1,512,64]{1,2,0:T(8,128)S(1)}, f32[1,512,1]{1,2,0:T(1,128)S(1)}, s32[]{:T(128)}, s32[]{:T(128)}, /*index=5*/bf16[1,2048,64]{2,1...) while((s32[]{:T(128)}, f32[1,512,64]{1,2,0:T(8,128)S(1)}, ...), condition=%wide.region_5.5_spmd.clone, body=%wide.region_1.4_spmd.clone.sunk | while | flops 109617672 | bytes 10115295 | solution.py:61
  147.1 1.9 fusion.42
  149.0 4.8 %fusion.43 = f32[1,512,4,128]{1,2,3,0:T(4,128)S(1)} fusion(f32[1,512,4,128]{1,3,2,0:T(8,128)S(1)} %bitcast.136), kind=kOutput, calls=%fused_computation.18.clone.1 | output fusion | flops 33292288 | bytes 2097152 | tf_op jit(solution)/shard_map/reduce-window
  154.2 1.6 fusion.44
  156.7 1.9 fusion.42
  158.6 4.8 %fusion.43 = f32[1,512,4,128]{1,2,3,0:T(4,128)S(1)} fusion(f32[1,512,4,128]{1,3,2,0:T(8,128)S(1)} %bitcast.136), kind=kOutput, calls=%fused_computation.18.clone.1 | output fusion | flops 33292288 | bytes 2097152 | tf_op jit(solution)/shard_map/reduce-window
  163.8 1.6 fusion.44
  171.1 28.9 %while.25 = (s32[]{:T(128)}, f32[1,512,64]{1,2,0:T(8,128)S(1)}, f32[1,512,1]{1,2,0:T(1,128)S(1)}, s32[]{:T(128)}, s32[]{:T(128)}, /*index=5*/bf16[1,2048,64]{2,1...) while((s32[]{:T(128)}, f32[1,512,64]{1,2,0:T(8,128)S(1)}, ...), condition=%wide.region_5.5_spmd.clone, body=%wide.region_1.4_spmd.clone.sunk | while | flops 109617672 | bytes 10115295 | solution.py:61
  171.7 1.9 fusion.42
  173.6 4.8 %fusion.43 = f32[1,512,4,128]{1,2,3,0:T(4,128)S(1)} fusion(f32[1,512,4,128]{1,3,2,0:T(8,128)S(1)} %bitcast.136), kind=kOutput, calls=%fused_computation.18.clone.1 | output fusion | flops 33292288 | bytes 2097152 | tf_op jit(solution)/shard_map/reduce-window
  178.8 1.6 fusion.44
  181.4 1.9 fusion.42
  183.2 4.8 %fusion.43 = f32[1,512,4,128]{1,2,3,0:T(4,128)S(1)} fusion(f32[1,512,4,128]{1,3,2,0:T(8,128)S(1)} %bitcast.136), kind=kOutput, calls=%fused_computation.18.clone.1 | output fusion | flops 33292288 | bytes 2097152 | tf_op jit(solution)/shard_map/reduce-window
  188.4 1.6 fusion.44
  191.0 1.9 fusion.42
  192.8 4.8 %fusion.43 = f32[1,512,4,128]{1,2,3,0:T(4,128)S(1)} fusion(f32[1,512,4,128]{1,3,2,0:T(8,128)S(1)} %bitcast.136), kind=kOutput, calls=%fused_computation.18.clone.1 | output fusion | flops 33292288 | bytes 2097152 | tf_op jit(solution)/shard_map/reduce-window
  198.1 1.6 fusion.44
  205.3 38.5 %while.25 = (s32[]{:T(128)}, f32[1,512,64]{1,2,0:T(8,128)S(1)}, f32[1,512,1]{1,2,0:T(1,128)S(1)}, s32[]{:T(128)}, s32[]{:T(128)}, /*index=5*/bf16[1,2048,64]{2,1...) while((s32[]{:T(128)}, f32[1,512,64]{1,2,0:T(8,128)S(1)}, ...), condition=%wide.region_5.5_spmd.clone, body=%wide.region_1.4_spmd.clone.sunk | while | flops 109617672 | bytes 10115295 | solution.py:61
  206.0 1.9 fusion.42
  207.8 4.8 %fusion.43 = f32[1,512,4,128]{1,2,3,0:T(4,128)S(1)} fusion(f32[1,512,4,128]{1,3,2,0:T(8,128)S(1)} %bitcast.136), kind=kOutput, calls=%fused_computation.18.clone.1 | output fusion | flops 33292288 | bytes 2097152 | tf_op jit(solution)/shard_map/reduce-window
  213.0 1.6 fusion.44
  215.6 1.9 fusion.42
  217.5 4.8 %fusion.43 = f32[1,512,4,128]{1,2,3,0:T(4,128)S(1)} fusion(f32[1,512,4,128]{1,3,2,0:T(8,128)S(1)} %bitcast.136), kind=kOutput, calls=%fused_computation.18.clone.1 | output fusion | flops 33292288 | bytes 2097152 | tf_op jit(solution)/shard_map/reduce-window
  225.2 1.9 fusion.42
  227.1 4.8 %fusion.43 = f32[1,512,4,128]{1,2,3,0:T(4,128)S(1)} fusion(f32[1,512,4,128]{1,3,2,0:T(8,128)S(1)} %bitcast.136), kind=kOutput, calls=%fused_computation.18.clone.1 | output fusion | flops 33292288 | bytes 2097152 | tf_op jit(solution)/shard_map/reduce-window
  234.8 1.9 fusion.42
  236.7 4.8 %fusion.43 = f32[1,512,4,128]{1,2,3,0:T(4,128)S(1)} fusion(f32[1,512,4,128]{1,3,2,0:T(8,128)S(1)} %bitcast.136), kind=kOutput, calls=%fused_computation.18.clone.1 | output fusion | flops 33292288 | bytes 2097152 | tf_op jit(solution)/shard_map/reduce-window
  247.4 11.8 %reduce.7 = bf16[2048,64]{1,0:T(8,128)(2,1)S(1)} reduce(bf16[2048,1,64]{2,1,0:T(2,128)(2,1)S(1)} %bitcast.140, bf16[]{:T(256)} %broadcast.71), dimensions={1}, to_apply=%bitcast.94.reduce_sub_computation | reduce | bytes 524290
  259.6 20.0 %all_to_all.69 = bf16[16,2,4096]{2,1,0:T(2,128)(2,1)S(1)} all-to-all(bf16[16,2,4096]{2,1,0:T(2,128)(2,1)S(1)} %reshape.174), channel_id=1, replica_groups=mesh['sp'=16,'dp'=32] {'sp'}, dimensions={0} | all-to-all | bytes 524288 | tf_op jit(solution)/shard_map/all_to_all | solution.py:113
  281.2 3.5 %fusion.24 = bf16[128,1024]{0,1:T(8,128)(2,1)S(1)} fusion(f32[1,128,16,64]{1,3,2,0:T(8,128)S(1)} %copy.87, bf16[2048,1024]{1,0:T(8,128)(2,1)} %all-gather.3.cloned.1.call-done, bf16[1,128,2048]{2,1,0:T(8,128)(2,1)S(1)} %copy-done), kind=kOutput, calls=%fused_computation.40 | convolution fusion | flops 537657344 | bytes 5505024 | tf_op jit(solution)/shard_map/dot_general | solution.py:99
  284.7 4.5 %fusion.22 = bf16[1,128,2048]{2,1,0:T(8,128)(2,1)} fusion(bf16[128,1024]{0,1:T(8,128)(2,1)S(1)} %fusion.24, bf16[1024,2048]{0,1:T(8,128)(2,1)} %all-gather.5.cloned.1.call-done), kind=kOutput, calls=%fused_computation.36 | convolution fusion | flops 537133056 | bytes 4980736 | tf_op jit(solution)/shard_map/dot_general | solution.py:115
  (152 shorter events, 38.7 us)
Async XLA Ops:
  6.5 274.7 %copy-start = (bf16[1,128,2048]{2,1,0:T(8,128)(2,1)S(1)}, bf16[1,128,2048]{2,1,0:T(8,128)(2,1)}, u32[]{:S(2)}) copy-start(bf16[1,128,2048]{2,1,0:T(8,128)(2,1)} %param.15) | copy-start | bytes 1572868
  6.5 64.4 %copy-start.1 = (bf16[1,128,1024]{2,1,0:T(8,128)(2,1)S(1)}, bf16[1,128,1024]{2,1,0:T(8,128)(2,1)}, u32[]{:S(2)}) copy-start(bf16[1,128,1024]{2,1,0:T(8,128)(2,1)} %param.11) | copy-start | bytes 786436
  6.5 84.4 %copy-start.2 = (bf16[1,128,1024]{2,1,0:T(8,128)(2,1)S(1)}, bf16[1,128,1024]{2,1,0:T(8,128)(2,1)}, u32[]{:S(2)}) copy-start(bf16[1,128,1024]{2,1,0:T(8,128)(2,1)} %param.12) | copy-start | bytes 786436
  6.5 274.6 %all-gather.3.cloned.1.call-start = ((), (), s32[]{:S(2)}) async-start(), calls=%async_computation.5 | async-start | bytes 4325376 | tf_op jit(solution)/shard_map/all_gather | solution.py:101
  45.1 19.9 %all-to-all-start.2 = ((bf16[1,128,16]{1,0,2:T(2,128)(2,1)}), bf16[1,128,16]{1,0,2:T(2,128)(2,1)S(1)}, u32[]{:S(2)}, u32[]{:S(2)}) async-start(bf16[1,128,16]{1,0,2:T(2,128)(2,1)} %copy.78), calls=%async_computation.2 | async-start | bytes 16384 | tf_op jit(solution)/shard_map/all_to_all | solution.py:110
  65.1 20.8 %all-to-all-start.3 = ((bf16[16,2,4096]{2,1,0:T(2,128)(2,1)}), bf16[16,2,4096]{2,1,0:T(2,128)(2,1)S(1)}, u32[]{:S(2)}, u32[]{:S(2)}) async-start(bf16[16,2,4096]{2,1,0:T(2,128)(2,1)} %reshape.172), calls=%async_computation.3 | async-start | bytes 524288 | tf_op jit(solution)/shard_map/all_to_all | solution.py:109
  85.8 19.8 %all-to-all-start = ((bf16[16,2,4096]{2,1,0:T(2,128)(2,1)}), bf16[16,2,4096]{2,1,0:T(2,128)(2,1)S(1)}, u32[]{:S(2)}, u32[]{:S(2)}) async-start(bf16[16,2,4096]{2,1,0:T(2,128)(2,1)} %reshape.168), calls=%async_computation | async-start | bytes 524288 | tf_op jit(solution)/shard_map/all_to_all | solution.py:107
  105.7 19.7 %all-to-all-start.1 = ((bf16[16,2,4096]{2,1,0:T(2,128)(2,1)}), bf16[16,2,4096]{2,1,0:T(2,128)(2,1)S(1)}, u32[]{:S(2)}, u32[]{:S(2)}) async-start(bf16[16,2,4096]{2,1,0:T(2,128)(2,1)} %reshape.170), calls=%async_computation.1 | async-start | bytes 524288 | tf_op jit(solution)/shard_map/all_to_all | solution.py:108
  110.9 173.8 %all-gather.5.cloned.1.call-start = ((), (), s32[]{:S(2)}) async-start(), calls=%async_computation.6 | async-start | bytes 4325376 | tf_op jit(solution)/shard_map/all_gather | solution.py:117
Sparse Core Ops, SparseCore 0:
  44.0 56.9 all-gather.2
  114.8 60.2 all-gather.4
where the time goes:
time: 297 us; the launch traced here: 296 us
  other arithmetic  84.9 us (29%)
  blocking collectives  54.6 us (18%)
  waiting for transfers between devices  40.2 us (14%)
  matrix products  29.4 us (10%)
  local copies, waits for them, and re-layouts  28.5 us (10%)
  starting transfers between devices  25.3 us (9%)
  loops' own time  19.6 us (7%)
  between operations  13.6 us (5%)
    another operation x20, other arithmetic  48.3 us
    all_gather x1, blocking collectives, turned_gather(): out = lax.all_gather(both, axis, axis=0, tiled=True)  34.7 us
    all_to_all x1, blocking collectives, shards(): lax.all_to_all(normed, 'sp', split_axis=1, concat_axis=2, tiled=True)  20 us
    unnamed x6, other arithmetic  18.8 us
    dot_general x10, matrix products, key_step(): jnp.einsum('gqd,gkd->gqk', query_block, key_block, preferred_element_type...  18.7 us
    convert_element_type x10, other arithmetic, key_step(): weights = jnp.where(earlier, jnp.exp(jax.nn.log_sigmoid(scores) + later_s...  15.7 us
    another operation x1, loops' own time, stick_blocks(): outputs = lax.map(one_block, jnp.arange(block_count, dtype=jnp.int32))  12.5 us
    all_to_all x1, waiting for transfers between devices, shards(): lax.all_to_all(value_rows, 'sp', split_axis=2, concat_axis=1, tiled=True)  11.4 us
  transfers between devices with their start and end apart: 6, of which 4 were waited for; matrix products, arithmetic and copies ran while one was open for 46% of the time, Pallas kernels for 0%

commit v1 on v0

v1 whole, which is shorter than its diff:
```python
import math
import jax
import jax.numpy as jnp
from jax import lax
from jax.experimental import pallas as pl
from jax.experimental.pallas import tpu as pltpu
from jax.sharding import PartitionSpec as P

eps_norm = 1e-05
log2e = math.log2(math.e)
score_cap = 25.0
f32, bf16 = jnp.float32, jnp.bfloat16
SRC, TOK, HD, GRP = 16, 128, 64, 4
ROWS = TOK + TOK // 2 + 8


def mm(a, b, ca=1, cb=0):
    return lax.dot_general(a, b, (((ca,), (cb,)), ((), ())), preferred_element_type=f32)


def pack_kernel(q_ref, k_ref, v_ref, o_ref, out_ref):
    row = lax.broadcasted_iota(jnp.int32, (TOK, TOK), 0)
    col = lax.broadcasted_iota(jnp.int32, (TOK, TOK), 1)
    perm = jnp.where(col == GRP * (row % 32) + row // 32, 1.0, 0.0).astype(bf16)
    keys = mm(perm, k_ref[0]).astype(bf16)
    vals = mm(perm, v_ref[0]).astype(bf16)
    offs = mm(o_ref[0], perm, 0, 1).astype(bf16)
    for h in range(SRC):
        s = slice(HD * h, HD * h + HD)
        out_ref[h, 0:TOK, :] = jnp.concatenate([q_ref[0, :, s], keys[:, s]], axis=1)
        out_ref[h, TOK:192, :] = jnp.concatenate([vals[0:64, s], vals[64:128, s]], axis=1)
        out_ref[h, 192:200, :] = jnp.broadcast_to(offs[h : h + 1, :], (8, TOK))


def pack(q, k, v, o):
    return pl.pallas_call(
        pack_kernel,
        out_shape=jax.ShapeDtypeStruct((SRC, ROWS, TOK), bf16),
    )(q, k, v, o)


def attn_kernel(buf_ref, out_ref, qq, kk, vv, of):
    nblk = SRC // GRP
    for i in range(SRC):
        q = buf_ref[i, 0:TOK, 0:HD].astype(f32) * (log2e / 8.0)
        hi = q.astype(bf16)
        lo = (q - hi.astype(f32)).astype(bf16)
        qq[TOK * i : TOK * i + TOK, :] = jnp.concatenate([hi, lo], axis=1)
        for g in range(GRP):
            k = buf_ref[i, 32 * g : 32 * g + 32, HD : 2 * HD]
            r = 512 * (i // 4) + 128 * g + 32 * (i % 4)
            kk[r : r + 32, :] = jnp.concatenate([k, k], axis=1)
            vr = TOK + 32 * (g % 2)
            vv[r : r + 32, :] = buf_ref[i, vr : vr + 32, HD * (g // 2) : HD * (g // 2) + HD]
    lane1 = lax.broadcasted_iota(jnp.int32, (8, TOK), 1)
    for b in range(nblk):
        rows = [buf_ref[4 * b + i, 192:200, :].astype(f32) * log2e for i in range(4)]
        for g in range(GRP):
            parts = [r if (i == g) else pltpu.roll(r, (32 * (i - g)) % TOK, 1) for i, r in enumerate(rows)]
            o = parts[3]
            for i in range(3):
                o = jnp.where(lane1 // 32 == i, parts[i], o)
            of[8 * (GRP * b + g) : 8 * (GRP * b + g) + 8, :] = o
    tr = lax.broadcasted_iota(jnp.int32, (256, 256), 0) % TOK
    tc = lax.broadcasted_iota(jnp.int32, (256, 256), 1)
    tri = jnp.where((tc >= TOK) | (tr > tc), -1.0, 0.0).astype(bf16)

    R = 256

    def block(qt, b, qrow, carry, acc, diag):
        ks = b * 512
        if not isinstance(b, int):
            ks = pl.multiple_of(ks, 512)
        x = mm(qt, kk[pl.ds(ks, 512), :], 1, 1)
        e, a = [], []
        for g in range(GRP):
            ob = b * 32 + 8 * g
            if not isinstance(b, int):
                ob = pl.multiple_of(ob, 8)
            off = of[pl.ds(ob, 8), :][0:1, :]
            eg = jnp.exp2(jnp.minimum(x[:, 128 * g : 128 * g + 128] - off, score_cap))
            if diag:
                m = lax.broadcasted_iota(jnp.int32, (R, TOK), 1)
                t = lax.broadcasted_iota(jnp.int32, (R, TOK), 0)
                eg = jnp.where(GRP * m + g < t + qrow, eg, 0.0)
            e.append(eg)
            a.append(1.0 + eg)
        lg = jnp.log2((a[0] * a[1]) * (a[2] * a[3]))
        hi = lg.astype(bf16)
        lo = (lg - hi.astype(f32)).astype(bf16)
        cc = mm(jnp.concatenate([hi, lo], axis=1), tri)
        t = jnp.exp2((cc[:, 0:TOK] + carry) - lg)
        carry = carry + cc[:, TOK:]
        w0 = e[0] * t
        t = t * a[0]
        w1 = e[1] * t
        t = t * a[1]
        w2 = e[2] * t
        t = t * a[2]
        w3 = e[3] * t
        w = jnp.concatenate([u.astype(bf16) for u in (w0, w1, w2, w3)], axis=1)
        acc = acc + mm(w, vv[pl.ds(ks, 512), :])
        return carry, acc

    for j in range(2048 // R):
        qt = qq[R * j : R * j + R, :]
        carry = jnp.zeros((R, TOK), f32)
        acc = jnp.zeros((R, HD), f32)
        db = (R * j) // 512
        carry, acc = block(qt, db, R * j - 512 * db, carry, acc, True)
        for b in range(db - 1, -1, -1):
            carry, acc = block(qt, b, 0, carry, acc, False)
        n = acc * lax.rsqrt(jnp.mean(acc * acc, axis=1, keepdims=True) + eps_norm)
        n = n.astype(bf16)
        for d in range(R // TOK):
            lo_, hi_ = n[TOK * d : TOK * d + 64], n[TOK * d + 64 : TOK * d + TOK]
            out_ref[(R // TOK) * j + d] = jnp.concatenate([lo_, hi_], axis=1)


def attend(buf):
    return pl.pallas_call(
        attn_kernel,
        out_shape=jax.ShapeDtypeStruct((SRC, 64, TOK), bf16),
        scratch_shapes=[
            pltpu.VMEM((2048, 128), bf16),
            pltpu.VMEM((2048, 128), bf16),
            pltpu.VMEM((2048, HD), bf16),
            pltpu.VMEM((128, TOK), f32),
        ],
        compiler_params=pltpu.CompilerParams(vmem_limit_bytes=48 * 1024 * 1024),
    )(buf)


def gate_kernel(h_ref, w_ref, out_ref, acc_ref):
    j = pl.program_id(0)
    w = w_ref[:, 0].reshape(256, 1024)
    part = mm(h_ref[0], w)

    @pl.when(j == 0)
    def _():
        acc_ref[...] = part

    @pl.when(j > 0)
    def _():
        acc_ref[...] += part

    @pl.when(j == pl.num_programs(0) - 1)
    def _():
        v = acc_ref[...]
        out_ref[...] = v / (1.0 + jnp.exp(-v))


def gate(hidden, w):
    return pl.pallas_call(
        gate_kernel,
        grid=(8,),
        in_specs=[
            pl.BlockSpec((1, TOK, 256), lambda j: (0, 0, j)),
            pl.BlockSpec((4, 1, 64, 1024), lambda j: (j, 0, 0, 0)),
        ],
        out_specs=pl.BlockSpec((TOK, 1024), lambda j: (0, 0)),
        out_shape=jax.ShapeDtypeStruct((TOK, 1024), f32),
        scratch_shapes=[pltpu.VMEM((TOK, 1024), f32)],
        cost_estimate=pl.CostEstimate(flops=2 * 128 * 1024 * 2048, bytes_accessed=5 << 20, transcendentals=1 << 17),
    )(hidden, w)


def mix_kernel(r_ref, g_ref, w_ref, out_ref, gd_ref):
    @pl.when(pl.program_id(0) == 0)
    def _():
        for h in range(0, SRC, 2):
            a, b = r_ref[h], r_ref[h + 1]
            top = jnp.concatenate([a[:, 0:HD], b[:, 0:HD]], axis=1)
            bot = jnp.concatenate([a[:, HD:], b[:, HD:]], axis=1)
            n = jnp.concatenate([top, bot], axis=0).astype(f32)
            s = slice(HD * h, HD * h + 2 * HD)
            gd_ref[:, s] = (n * g_ref[:, s]).astype(bf16)

    w = w_ref[:, 0].reshape(256, 1024)
    out_ref[0] = mm(gd_ref[...], w, 1, 1).astype(bf16)


def mix(ret, gact, w):
    return pl.pallas_call(
        mix_kernel,
        grid=(8,),
        in_specs=[
            pl.BlockSpec((SRC, 64, TOK), lambda j: (0, 0, 0)),
            pl.BlockSpec((TOK, 1024), lambda j: (0, 0)),
            pl.BlockSpec((4, 1, 64, 1024), lambda j: (j, 1, 0, 0)),
        ],
        out_specs=pl.BlockSpec((1, TOK, 256), lambda j: (0, 0, j)),
        out_shape=jax.ShapeDtypeStruct((1, TOK, 2048), bf16),
        scratch_shapes=[pltpu.VMEM((TOK, 1024), bf16)],
        cost_estimate=pl.CostEstimate(flops=2 * 128 * 1024 * 2048, bytes_accessed=6 << 20, transcendentals=0),
    )(ret, gact, w)


def turn_kernel(x_ref, out_ref):
    out_ref[...] = x_ref[...].T


def turn(x):
    return pl.pallas_call(turn_kernel, out_shape=jax.ShapeDtypeStruct((128, 1024), bf16))(x)


def shards(queries, key_rows, value_rows, break_offset, hidden_in, gate_weight, out_weight):
    own = jnp.concatenate([gate_weight.T, out_weight], axis=1)
    cols = turn(lax.all_gather(own, "sp", axis=0, tiled=True))
    w = lax.all_gather(cols[None], "dp", axis=0, tiled=True).reshape(32, 2, 64, 1024)
    buf = pack(queries, key_rows, value_rows, break_offset)
    buf = lax.all_to_all(buf, "sp", split_axis=0, concat_axis=0, tiled=True)
    heads = attend(buf)
    ret = lax.all_to_all(heads, "sp", split_axis=0, concat_axis=0, tiled=True)
    return mix(ret, gate(hidden_in, w), w)


def solution(mesh):
    tok = P("dp", "sp", None)
    return jax.shard_map(
        shards,
        mesh=mesh,
        in_specs=(tok, tok, tok, tok, tok, P("dp", "sp"), P("sp", "dp")),
        out_specs=tok,
        check_vma=False,
    )
```

time: 297 us -> 141 us (0.47)
  the two profiles are of different devices: /device:TPU:54 before, /device:TPU:30 now
where the time goes in v1:
time: 141 us; the launch traced here: 140 us
  blocking collectives  80.6 us (57%)
  Pallas kernels  26.8 us (19%)
  between operations  13.4 us (10%)
  waiting for transfers between devices  9.67 us (7%)
  starting transfers between devices  6.25 us (4%)
  local copies, waits for them, and re-layouts  2.93 us (2%)
    all_to_all x1, blocking collectives, shards(): buf = lax.all_to_all(buf, 'sp', split_axis=0, concat_axis=0, tiled=True)  41.4 us
    all_gather x1, blocking collectives, shards(): cols = turn(lax.all_gather(own, 'sp', axis=0, tiled=True))  39.2 us
    pallas_call x1, Pallas kernels, attend(): pl.pallas_call(attn_kernel, out_shape=jax.ShapeDtypeStruct((SRC, 64, TOK)...  8.51 us
    all_to_all x1, waiting for transfers between devices, shards(): ret = lax.all_to_all(heads, 'sp', split_axis=0, concat_axis=0, tiled=True)  7.84 us
    pallas_call x1, Pallas kernels, mix(): pl.pallas_call(mix_kernel, grid=(8,), in_specs=[pl.BlockSpec((SRC, 64, TO...  7.24 us
    pallas_call x1, Pallas kernels, gate(): pl.pallas_call(gate_kernel, grid=(8,), in_specs=[pl.BlockSpec((1, TOK, 25...  6.85 us
    all_to_all x1, starting transfers between devices, shards(): ret = lax.all_to_all(heads, 'sp', split_axis=0, concat_axis=0, tiled=True)  6.24 us
    unnamed x4, local copies, waits for them, and re-layouts  2.93 us
  transfers between devices with their start and end apart: 2, of which 2 were waited for; matrix products, arithmetic and copies ran while one was open for 1% of the time, Pallas kernels for 13%

profile of v1, /device:TPU:30, one launch (start us, length us, event | category | flops | bytes accessed | tf_op | source)
XLA Modules:
  0.0 140.5 jit_solution(13040247338947500910)
XLA Ops:
  6.5 0.0 all-gather.3.cloned.1.call-start
  6.5 0.8 copy.9
  7.3 0.8 pad_maximum_fusion
  8.1 39.2 %all_gather.6.x_ref = bf16[1024,128]{1,0:T(8,128)(2,1)} all-gather(bf16[64,128]{1,0:T(8,128)(2,1)S(1)} %pad_maximum_fusion), channel_id=1, replica_groups=mesh['sp'=16,'dp'=32] {'sp'}, dimensions={0}, use_global_device_ids=true | all-gather | bytes 278528 | tf_op jit(solution)/shard_map/all_gather | solution.py:209
  47.4 1.8 %shard_map.75 = bf16[128,1024]{1,0:T(8,128)(2,1)} custom-call(bf16[1024,128]{1,0:T(8,128)(2,1)} %all_gather.6.x_ref), custom_call_target="tpu_custom_call" | custom-call | tf_op jit(solution)/shard_map/pallas_call | solution.py:204
  49.2 0.0 all-gather.3.cloned.1.call-update
  49.2 1.4 %copy.8.o_ref = bf16[1,128,16]{2,1,0:T(8,128)(2,1)} copy(bf16[1,128,16]{1,2,0:T(8,128)(2,1)} %param.10) | data formatting | bytes 8192 | tf_op args[3]
  50.6 2.4 %shard_map.73 = bf16[16,200,128]{2,1,0:T(8,128)(2,1)} custom-call(bf16[1,128,1024]{2,1,0:T(8,128)(2,1)} %q_ref.1, bf16[1,128,1024]{2,1,0:T(8,128)(2,1)} %k_ref.1, bf16[1,128,1024]{2,1,0:T(8,128)(2,1)} %v_ref.1, bf16[1,128,16]{2,1,0:T(8,128)(2,1)} %copy.8.o_ref), custom_call_target="tpu_custom_call" | custom-call | tf_op jit(solution)/shard_map/pallas_call | solution.py:36
  53.0 41.4 %all_to_all.10.buf_ref = bf16[16,200,128]{2,1,0:T(8,128)(2,1)S(1)} all-to-all(bf16[16,200,128]{2,1,0:T(8,128)(2,1)} %shard_map.73), channel_id=1, replica_groups=mesh['sp'=16,'dp'=32] {'sp'}, dimensions={0} | all-to-all | bytes 1638400 | tf_op jit(solution)/shard_map/all_to_all | solution.py:212
  94.4 8.5 %shard_map.74 = bf16[16,64,128]{2,1,0:T(8,128)(2,1)} custom-call(bf16[16,200,128]{2,1,0:T(8,128)(2,1)S(1)} %all_to_all.10.buf_ref), custom_call_target="tpu_custom_call" | custom-call | tf_op jit(solution)/shard_map/pallas_call | solution.py:121
  102.9 6.2 %all-to-all-start.1 = ((bf16[16,64,128]{2,1,0:T(8,128)(2,1)}), bf16[16,64,128]{2,1,0:T(8,128)(2,1)S(1)}, u32[]{:S(2)}, u32[]{:S(2)}) async-start(bf16[16,64,128]{2,1,0:T(8,128)(2,1)} %shard_map.74), calls=%async_computation.1 | async-start | bytes 524288 | tf_op jit(solution)/shard_map/all_to_all | solution.py:214
  109.1 1.8 %all-gather.3.cloned.1.call-done = bf16[4096,1024]{1,0:T(8,128)(2,1)} async-done(((bf16[128,1024]{1,0:T(8,128)(2,1)}), bf16[4096,1024]{1,0:T(8,128)(2,1)}) %all-gather.3.cloned.1.call-update) | async-done | bytes 8388624 | tf_op jit(solution)/shard_map/all_gather | solution.py:210
  111.0 6.9 %shard_map.76.g_ref = f32[128,1024]{1,0:T(8,128)} custom-call(bf16[1,128,2048]{2,1,0:T(8,128)(2,1)} %h_ref.1, bf16[32,2,64,1024]{3,2,1,0:T(8,128)(2,1)} %bitcast.2), custom_call_target="tpu_custom_call" | custom-call | flops 536870912 | bytes 5242880 | tf_op jit(solution)/shard_map/pallas_call | solution.py:154
  117.8 7.8 %all-to-all-done.1.r_ref = bf16[16,64,128]{2,1,0:T(8,128)(2,1)S(1)} async-done(((bf16[16,64,128]{2,1,0:T(8,128)(2,1)}), bf16[16,64,128]{2,1,0:T(8,128)(2,1)S(1)}, u32[]{:S(2)}, u32[]{:S(2)}) %all-to-all-start.1) | async-done | bytes 262176 | tf_op jit(solution)/shard_map/all_to_all | solution.py:214
  125.7 0.0 copy-start
  125.7 0.7 copy-done
  126.4 7.2 %shard_map.77 = bf16[1,128,2048]{2,1,0:T(8,128)(2,1)} custom-call(bf16[16,64,128]{2,1,0:T(8,128)(2,1)} %copy-done, f32[128,1024]{1,0:T(8,128)} %shard_map.76.g_ref, bf16[32,2,64,1024]{3,2,1,0:T(8,128)(2,1)} %bitcast.3), custom_call_target="tpu_custom_call" | custom-call | flops 536870912 | bytes 6291456 | tf_op jit(solution)/shard_map/pallas_call | solution.py:184
Async XLA Ops:
  6.5 104.4 %all-gather.3.cloned.1.call-start = ((), (), s32[]{:S(2)}) async-start(), calls=%async_computation.2 | async-start | bytes 8650752 | tf_op jit(solution)/shard_map/all_gather | solution.py:210
  102.9 22.8 %all-to-all-start.1 = ((bf16[16,64,128]{2,1,0:T(8,128)(2,1)}), bf16[16,64,128]{2,1,0:T(8,128)(2,1)S(1)}, u32[]{:S(2)}, u32[]{:S(2)}) async-start(bf16[16,64,128]{2,1,0:T(8,128)(2,1)} %shard_map.74), calls=%async_computation.1 | async-start | bytes 524288 | tf_op jit(solution)/shard_map/all_to_all | solution.py:214
  125.7 0.7 copy-start
Sparse Core Ops, SparseCore 0:
  49.3 61.6 all-gather.2

commit v2 on v1

--- a/solution.py
+++ b/solution.py
@@ -5,6 +5,7 @@
 from jax.experimental import pallas as pl
 from jax.experimental.pallas import tpu as pltpu
 from jax.sharding import PartitionSpec as P
+
 
 eps_norm = 1e-05
 log2e = math.log2(math.e)
@@ -131,88 +132,113 @@
     )(buf)
 
 
-def gate_kernel(h_ref, w_ref, out_ref, acc_ref):
-    j = pl.program_id(0)
-    w = w_ref[:, 0].reshape(256, 1024)
-    part = mm(h_ref[0], w)
-
-    @pl.when(j == 0)
-    def _():
-        acc_ref[...] = part
-
-    @pl.when(j > 0)
-    def _():
-        acc_ref[...] += part
-
-    @pl.when(j == pl.num_programs(0) - 1)
-    def _():
-        v = acc_ref[...]
-        out_ref[...] = v / (1.0 + jnp.exp(-v))
-
-
-def gate(hidden, w):
+def turn_kernel(x_ref, out_ref):
+    out_ref[...] = x_ref[...].T
+
+
+def turn(x):
+    return pl.pallas_call(turn_kernel, out_shape=jax.ShapeDtypeStruct((128, 1024), bf16))(x)
+
+
+def two_chips(pos_ref, own_ref, sib_ref, j):
+    p = pos_ref[0]
+    south, x, y = (p & 1) == 0, (p >> 1) & 3, p >> 3
+    rows = []
+    for chip in (2 * j, 2 * j + 1):
+        dy, dx = (y - chip // 4) & 3, (x - chip % 4) & 3
+        first, second = 4 * dy + dx, 4 * dx + dy
+        a = own_ref[jnp.where(south, first, second)]
+        b = sib_ref[jnp.where(south, second, first)]
+        rows += [jnp.where(south, a, b), jnp.where(south, b, a)]
+    return jnp.concatenate(rows, axis=0)
+
+
+def gate_kernel(pos_ref, h_ref, own_ref, sib_ref, out_ref):
+    acc = jnp.zeros((TOK, 1024), f32)
+    for j in range(8):
+        acc = acc + mm(h_ref[0, :, 256 * j : 256 * j + 256], two_chips(pos_ref, own_ref, sib_ref, j))
+    out_ref[...] = acc / (1.0 + jnp.exp(-acc))
+
+
+def mix_kernel(pos_ref, r_ref, g_ref, own_ref, sib_ref, out_ref, gd_ref):
+    for h in range(0, SRC, 2):
+        a, b = r_ref[h], r_ref[h + 1]
+        top = jnp.concatenate([a[:, 0:HD], b[:, 0:HD]], axis=1)
+        bot = jnp.concatenate([a[:, HD:], b[:, HD:]], axis=1)
+        n = jnp.concatenate([top, bot], axis=0).astype(f32)
+        s = slice(HD * h, HD * h + 2 * HD)
+        gd_ref[:, s] = (n * g_ref[:, s]).astype(bf16)
+    for j in range(8):
+        w = two_chips(pos_ref, own_ref, sib_ref, j)
+        out_ref[0, :, 256 * j : 256 * j + 256] = mm(gd_ref[...], w, 1, 1).astype(bf16)
+
+
+def whole(n, smem=1):
+    spec = [pl.BlockSpec(memory_space=pltpu.SMEM)] * smem
+    return spec + [pl.BlockSpec(memory_space=pltpu.VMEM)] * n
+
+
+def gate(tab, hidden, own, sib):
     return pl.pallas_call(
         gate_kernel,
-        grid=(8,),
-        in_specs=[
-            pl.BlockSpec((1, TOK, 256), lambda j: (0, 0, j)),
-            pl.BlockSpec((4, 1, 64, 1024), lambda j: (j, 0, 0, 0)),
-        ],
-        out_specs=pl.BlockSpec((TOK, 1024), lambda j: (0, 0)),
+        in_specs=whole(3),
         out_shape=jax.ShapeDtypeStruct((TOK, 1024), f32),
-        scratch_shapes=[pltpu.VMEM((TOK, 1024), f32)],
+        compiler_params=pltpu.CompilerParams(vmem_limit_bytes=40 * 1024 * 1024),
         cost_estimate=pl.CostEstimate(flops=2 * 128 * 1024 * 2048, bytes_accessed=5 << 20, transcendentals=1 << 17),
-    )(hidden, w)
-
-
-def mix_kernel(r_ref, g_ref, w_ref, out_ref, gd_ref):
-    @pl.when(pl.program_id(0) == 0)
-    def _():
-        for h in range(0, SRC, 2):
-            a, b = r_ref[h], r_ref[h + 1]
-            top = jnp.concatenate([a[:, 0:HD], b[:, 0:HD]], axis=1)
-            bot = jnp.concatenate([a[:, HD:], b[:, HD:]], axis=1)
-            n = jnp.concatenate([top, bot], axis=0).astype(f32)
-            s = slice(HD * h, HD * h + 2 * HD)
-            gd_ref[:, s] = (n * g_ref[:, s]).astype(bf16)
-
-    w = w_ref[:, 0].reshape(256, 1024)
-    out_ref[0] = mm(gd_ref[...], w, 1, 1).astype(bf16)
-
-
-def mix(ret, gact, w):
+    )(tab, hidden, own, sib)
+
+
+def mix(tab, ret, gact, own, sib):
     return pl.pallas_call(
         mix_kernel,
-        grid=(8,),
-        in_specs=[
-            pl.BlockSpec((SRC, 64, TOK), lambda j: (0, 0, 0)),
-            pl.BlockSpec((TOK, 1024), lambda j: (0, 0)),
-            pl.BlockSpec((4, 1, 64, 1024), lambda j: (j, 1, 0, 0)),
-        ],
-        out_specs=pl.BlockSpec((1, TOK, 256), lambda j: (0, 0, j)),
+        in_specs=whole(4),
         out_shape=jax.ShapeDtypeStruct((1, TOK, 2048), bf16),
         scratch_shapes=[pltpu.VMEM((TOK, 1024), bf16)],
+        compiler_params=pltpu.CompilerParams(vmem_limit_bytes=40 * 1024 * 1024),
         cost_estimate=pl.CostEstimate(flops=2 * 128 * 1024 * 2048, bytes_accessed=6 << 20, transcendentals=0),
-    )(ret, gact, w)
-
-
-def turn_kernel(x_ref, out_ref):
-    out_ref[...] = x_ref[...].T
-
-
-def turn(x):
-    return pl.pallas_call(turn_kernel, out_shape=jax.ShapeDtypeStruct((128, 1024), bf16))(x)
+    )(tab, ret, gact, own, sib)
+
+
+def moves(phase, step):
+    out = []
+    for y in range(4):
+        for x in range(4):
+            for c in range(2):
+                along_x = (c == 0) == (phase == 1)
+                ty, tx = (y, (x + step) % 4) if along_x else ((y + step) % 4, x)
+                out.append(((y * 4 + x) * 2 + c, (ty * 4 + tx) * 2 + c))
+    return out
+
+
+def ring(b, phase):
+    back1 = lax.ppermute(b, "dp", moves(phase, 1))
+    back3 = lax.ppermute(b, "dp", moves(phase, -1))
+    top = lax.ppermute(b[..., :64, :], "dp", moves(phase, 2))
+    bot = lax.ppermute(b[..., 64:, :], "dp", moves(phase, -2))
+    return back1, back3, top, bot
 
 
 def shards(queries, key_rows, value_rows, break_offset, hidden_in, gate_weight, out_weight):
-    own = jnp.concatenate([gate_weight.T, out_weight], axis=1)
-    cols = turn(lax.all_gather(own, "sp", axis=0, tiled=True))
-    w = lax.all_gather(cols[None], "dp", axis=0, tiled=True).reshape(32, 2, 64, 1024)
     buf = pack(queries, key_rows, value_rows, break_offset)
+    joined = jnp.concatenate([gate_weight.T, out_weight], axis=1)
+    buf, joined = lax.optimization_barrier((buf, joined))
+    joined = lax.all_gather(joined, "sp", axis=0, tiled=True)
+    buf, joined = lax.optimization_barrier((buf, joined))
     buf = lax.all_to_all(buf, "sp", split_axis=0, concat_axis=0, tiled=True)
+    b = turn(joined)
+    back1, back3, top, bot = ring(b, 1)
+    b = jnp.stack([b, back1, jnp.concatenate([top, bot], axis=0), back3])
+    back1, back3, top, bot = ring(b, 2)
+    own_g = jnp.concatenate([b[:, :64], back1[:, :64], top, back3[:, :64]], axis=0)
+    own_o = jnp.concatenate([b[:, 64:], back1[:, 64:], bot, back3[:, 64:]], axis=0)
+    swap = [(p, p ^ 1) for p in range(32)]
+    sib_g = lax.ppermute(own_g, "dp", swap)
+    sib_o = lax.ppermute(own_o, "dp", swap)
+    pos = lax.axis_index("dp").astype(jnp.int32).reshape(1)
     heads = attend(buf)
     ret = lax.all_to_all(heads, "sp", split_axis=0, concat_axis=0, tiled=True)
-    return mix(ret, gate(hidden_in, w), w)
+    gact = gate(pos, hidden_in, own_g, sib_g)
+    return mix(pos, ret, gact, own_o, sib_o)
 
 
 def solution(mesh):

time: 141 us -> 153 us (1.085)
  the two profiles are of different devices: /device:TPU:30 before, /device:TPU:6 now
where the time goes in v2:
time: 153 us
  starting transfers between devices  51.6 us (34%)
  blocking collectives  39.2 us (26%)
  waiting for transfers between devices  35.6 us (23%)
  Pallas kernels  19.6 us (13%)
  local copies, waits for them, and re-layouts  3.51 us (2%)
  other arithmetic  2.8 us (2%)
    all_gather x1, blocking collectives, shards(): joined = lax.all_gather(joined, 'sp', axis=0, tiled=True)  39.2 us
    all_to_all x1, waiting for transfers between devices, shards(): ret = lax.all_to_all(heads, 'sp', split_axis=0, concat_axis=0, tiled=True)  16 us
    ppermute x2, waiting for transfers between devices, ring(): back3 = lax.ppermute(b, 'dp', moves(phase, -1))  14.1 us
    all_to_all x1, starting transfers between devices, shards(): ret = lax.all_to_all(heads, 'sp', split_axis=0, concat_axis=0, tiled=True)  12 us
    ppermute x2, starting transfers between devices, ring(): top = lax.ppermute(b[..., :64, :], 'dp', moves(phase, 2))  9.36 us
    pallas_call x1, Pallas kernels, attend(): pl.pallas_call(attn_kernel, out_shape=jax.ShapeDtypeStruct((SRC, 64, TOK)...  8.52 us
    ppermute x2, starting transfers between devices, ring(): back3 = lax.ppermute(b, 'dp', moves(phase, -1))  7.78 us
    all_to_all x1, starting transfers between devices, shards(): buf = lax.all_to_all(buf, 'sp', split_axis=0, concat_axis=0, tiled=True)  6.61 us
  transfers between devices with their start and end apart: 12, of which 3 were waited for; matrix products, arithmetic and copies ran while one was open for 2% of the time, Pallas kernels for 7%

profile of v2, /device:TPU:6, one launch (start us, length us, event | category | flops | bytes accessed | tf_op | source)
XLA Modules:
  0.0 152.7 jit_solution(840081837858013776)
XLA Ops:
  0.0 1.4 copy.8.o_ref
  1.4 0.8 copy.9
  2.2 0.8 pad_maximum_fusion.3
  3.0 2.4 %shard_map.73 = bf16[16,200,128]{2,1,0:T(8,128)(2,1)} custom-call(bf16[1,128,1024]{2,1,0:T(8,128)(2,1)} %q_ref.1, bf16[1,128,1024]{2,1,0:T(8,128)(2,1)} %k_ref.1, bf16[1,128,1024]{2,1,0:T(8,128)(2,1)} %v_ref.1, bf16[1,128,16]{2,1,0:T(8,128)(2,1)} %copy.8.o_ref), custom_call_target="tpu_custom_call" | custom-call | tf_op jit(solution)/shard_map/pallas_call | solution.py:37
  5.4 39.2 %all_gather.3.x_ref = bf16[1024,128]{1,0:T(8,128)(2,1)} all-gather(bf16[64,128]{1,0:T(8,128)(2,1)S(1)} %pad_maximum_fusion.3), channel_id=1, replica_groups=mesh['sp'=16,'dp'=32] {'sp'}, dimensions={0}, use_global_device_ids=true | all-gather | bytes 278528 | tf_op jit(solution)/shard_map/all_gather | solution.py:225
  44.6 1.8 %shard_map.75 = bf16[128,1024]{1,0:T(8,128)(2,1)} custom-call(bf16[1024,128]{1,0:T(8,128)(2,1)} %all_gather.3.x_ref), custom_call_target="tpu_custom_call" | custom-call | tf_op jit(solution)/shard_map/pallas_call | solution.py:140
  46.4 0.0 copy-start.1
  46.4 2.9 %collective-permute-start.3 = (bf16[128,1024]{1,0:T(8,128)(2,1)}, bf16[128,1024]{1,0:T(8,128)(2,1)S(1)}, u32[]{:S(2)}, u32[]{:S(2)}) collective-permute-start(bf16[128,1024]{1,0:T(8,128)(2,1)} %shard_map.75), channel_id=1, source_target_pairs={{0,6},{1,25},{2,0},{3,27},{4,2},{5,29},{6,4},{7,31},{8,14},{9,1},{... | collective-permute-start | bytes 786440 | tf_op jit(solution)/shard_map/ppermute | solution.py:215
  49.3 4.3 %collective-permute-start = (bf16[128,1024]{1,0:T(8,128)(2,1)}, bf16[128,1024]{1,0:T(8,128)(2,1)S(1)}, u32[]{:S(2)}, u32[]{:S(2)}) collective-permute-start(bf16[128,1024]{1,0:T(8,128)(2,1)} %shard_map.75), channel_id=1, source_target_pairs={{0,2},{1,9},{2,4},{3,11},{4,6},{5,13},{6,0},{7,15},{8,10},{9,17},{... | collective-permute-start | bytes 786440 | tf_op jit(solution)/shard_map/ppermute | solution.py:214
  53.6 1.0 fusion.3
  54.6 2.1 %collective-permute-start.2 = (bf16[64,1024]{1,0:T(8,128)(2,1)S(1)}, bf16[64,1024]{1,0:T(8,128)(2,1)S(1)}, u32[]{:S(2)}, u32[]{:S(2)}) collective-permute-start(bf16[64,1024]{1,0:T(8,128)(2,1)S(1)} %get-tuple-element.20), channel_id=1, source_target_pairs={{0,4},{1,17},{2,6},{3,19},{4,0},{5,21},{6,2},{7,23},{8,12},{9,25},... | collective-permute-start | bytes 393224 | tf_op jit(solution)/shard_map/ppermute | solution.py:217
  56.7 5.3 %collective-permute-start.1 = (bf16[64,1024]{1,0:T(8,128)(2,1)S(1)}, bf16[64,1024]{1,0:T(8,128)(2,1)S(1)}, u32[]{:S(2)}, u32[]{:S(2)}) collective-permute-start(bf16[64,1024]{1,0:T(8,128)(2,1)S(1)} %get-tuple-element.19), channel_id=1, source_target_pairs={{0,4},{1,17},{2,6},{3,19},{4,0},{5,21},{6,2},{7,23},{8,12},{9,25},... | collective-permute-start | bytes 393224 | tf_op jit(solution)/shard_map/ppermute | solution.py:216
  62.0 6.6 %all-to-all-start = ((bf16[16,200,128]{2,1,0:T(8,128)(2,1)}), bf16[16,200,128]{2,1,0:T(8,128)(2,1)S(1)}, u32[]{:S(2)}, u32[]{:S(2)}) async-start(bf16[16,200,128]{2,1,0:T(8,128)(2,1)} %shard_map.73), calls=%async_computation | async-start | bytes 1638400 | tf_op jit(solution)/shard_map/all_to_all | solution.py:227
  68.6 0.0 collective-permute-done.2
  68.6 0.0 collective-permute-done.1
  68.6 0.0 collective-permute-done.3
  68.6 0.0 collective-permute-done
  68.6 0.0 copy-done.1
  68.7 0.1 pad_maximum_fusion.2
  68.8 4.9 %collective-permute-start.6 = (bf16[4,128,1024]{2,1,0:T(8,128)(2,1)S(1)}, bf16[4,128,1024]{2,1,0:T(8,128)(2,1)S(1)}, u32[]{:S(2)}, u32[]{:S(2)}) collective-permute-start(bf16[4,128,1024]{2,1,0:T(8,128)(2,1)S(1)} %pad_maximum_fusion.2), channel_id=1, source_target_pairs={{0,24},{1,7},{2,26},{3,1},{4,28},{5,3},{6,30},{7,5},{8,0},{9,15},{... | collective-permute-start | bytes 3145736 | tf_op jit(solution)/shard_map/ppermute | solution.py:215
  73.7 1.9 %collective-permute-start.4 = (bf16[4,128,1024]{2,1,0:T(8,128)(2,1)S(1)}, bf16[4,128,1024]{2,1,0:T(8,128)(2,1)S(1)}, u32[]{:S(2)}, u32[]{:S(2)}) collective-permute-start(bf16[4,128,1024]{2,1,0:T(8,128)(2,1)S(1)} %pad_maximum_fusion.2), channel_id=1, source_target_pairs={{0,8},{1,3},{2,10},{3,5},{4,12},{5,7},{6,14},{7,1},{8,16},{9,11},{... | collective-permute-start | bytes 3145736 | tf_op jit(solution)/shard_map/ppermute | solution.py:214
  75.7 0.1 fusion.1
  75.8 4.1 %collective-permute-start.5 = (bf16[4,64,1024]{2,1,0:T(8,128)(2,1)S(1)}, bf16[4,64,1024]{2,1,0:T(8,128)(2,1)S(1)}, u32[]{:S(2)}, u32[]{:S(2)}) collective-permute-start(bf16[4,64,1024]{2,1,0:T(8,128)(2,1)S(1)} %get-tuple-element.16), channel_id=1, source_target_pairs={{0,16},{1,5},{2,18},{3,7},{4,20},{5,1},{6,22},{7,3},{8,24},{9,13},... | collective-permute-start | bytes 1572872 | tf_op jit(solution)/shard_map/ppermute | solution.py:216
  79.9 3.2 %collective-permute-start.8 = (bf16[4,64,1024]{2,1,0:T(8,128)(2,1)S(1)}, bf16[4,64,1024]{2,1,0:T(8,128)(2,1)S(1)}, u32[]{:S(2)}, u32[]{:S(2)}) collective-permute-start(bf16[4,64,1024]{2,1,0:T(8,128)(2,1)S(1)} %get-tuple-element.15), channel_id=1, source_target_pairs={{0,16},{1,5},{2,18},{3,7},{4,20},{5,1},{6,22},{7,3},{8,24},{9,13},... | collective-permute-start | bytes 1572872 | tf_op jit(solution)/shard_map/ppermute | solution.py:217
  83.1 14.1 %collective-permute-done.6 = bf16[4,128,1024]{2,1,0:T(8,128)(2,1)S(1)} collective-permute-done((bf16[4,128,1024]{2,1,0:T(8,128)(2,1)S(1)}, bf16[4,128,1024]{2,1,0:T(8,128)(2,1)S(1)}, u32[]{:S(2)}, u32[]{:S(2)}) %collective-permute-start.6) | collective-permute-done | bytes 1048608 | tf_op jit(solution)/shard_map/ppermute | solution.py:215
  97.3 0.1 fusion.2
  97.4 5.5 %collective-permute-done.4 = bf16[4,128,1024]{2,1,0:T(8,128)(2,1)S(1)} collective-permute-done((bf16[4,128,1024]{2,1,0:T(8,128)(2,1)S(1)}, bf16[4,128,1024]{2,1,0:T(8,128)(2,1)S(1)}, u32[]{:S(2)}, u32[]{:S(2)}) %collective-permute-start.4) | collective-permute-done | bytes 1048608 | tf_op jit(solution)/shard_map/ppermute | solution.py:214
  102.9 0.1 fusion
  103.0 0.0 collective-permute-done.5
  103.0 0.3 pad_maximum_fusion.own_ref
  103.3 1.9 %collective-permute-start.7 = (bf16[16,64,1024]{2,1,0:T(8,128)(2,1)S(1)}, bf16[16,64,1024]{2,1,0:T(8,128)(2,1)}, u32[]{:S(2)}, u32[]{:S(2)}) collective-permute-start(bf16[16,64,1024]{2,1,0:T(8,128)(2,1)S(1)} %pad_maximum_fusion.own_ref), channel_id=1, source_target_pairs={{0,1},{1,0},{2,3},{3,2},{4,5},{5,4},{6,7},{7,6},{8,9},{9,8},{10,11... | collective-permute-start | bytes 6291464 | tf_op jit(solution)/shard_map/ppermute | solution.py:235
  105.2 0.0 collective-permute-done.8
  105.2 0.0 copy-start
  105.2 1.6 %pad_maximum_fusion.1.own_ref = bf16[16,64,1024]{2,1,0:T(8,128)(2,1)} fusion(bf16[4,64,1024]{2,1,0:T(8,128)(2,1)S(1)} %get-tuple-element.17, bf16[4,64,1024]{2,1,0:T(8,128)(2,1)S(1)} %collective-permute-done.8, bf16[4,64,1024]{2,1,0:T(8,128)(2,1)S(1)} %get-tuple-element.13, bf16[4,64,1024]{2,1,0:T(8,128)(2,1)S(1)} %get-tuple-element.15), kind=kLoop, calls=%fused_computation.1 | loop fusion | flops 3145728 | bytes 4194304 | tf_op jit(solution)/shard_map/concatenate | solution.py:233
  106.8 2.4 %collective-permute-start.9 = (bf16[16,64,1024]{2,1,0:T(8,128)(2,1)}, bf16[16,64,1024]{2,1,0:T(8,128)(2,1)}, u32[]{:S(2)}, u32[]{:S(2)}) collective-permute-start(bf16[16,64,1024]{2,1,0:T(8,128)(2,1)} %pad_maximum_fusion.1.own_ref), channel_id=1, source_target_pairs={{0,1},{1,0},{2,3},{3,2},{4,5},{5,4},{6,7},{7,6},{8,9},{9,8},{10,11... | collective-permute-start | bytes 6291464 | tf_op jit(solution)/shard_map/ppermute | solution.py:236
  109.2 0.0 all-to-all-done.buf_ref
  109.2 8.5 %shard_map.74 = bf16[16,64,128]{2,1,0:T(8,128)(2,1)} custom-call(bf16[16,200,128]{2,1,0:T(8,128)(2,1)S(1)} %all-to-all-done.buf_ref), custom_call_target="tpu_custom_call" | custom-call | tf_op jit(solution)/shard_map/pallas_call | solution.py:122
  117.7 12.0 %all-to-all-start.1 = ((bf16[16,64,128]{2,1,0:T(8,128)(2,1)}), bf16[16,64,128]{2,1,0:T(8,128)(2,1)S(1)}, u32[]{:S(2)}, u32[]{:S(2)}) async-start(bf16[16,64,128]{2,1,0:T(8,128)(2,1)} %shard_map.74), calls=%async_computation.1 | async-start | bytes 524288 | tf_op jit(solution)/shard_map/all_to_all | solution.py:239
  129.7 0.0 collective-permute-done.7.sib_ref
  129.8 0.0 copy-done
  129.8 2.4 %shard_map.76.g_ref = f32[128,1024]{1,0:T(8,128)S(1)} custom-call(s32[1]{0:T(128)} %bitcast.pos_ref, bf16[1,128,2048]{2,1,0:T(8,128)(2,1)S(1)} %copy-done, bf16[16,64,1024]{2,1,0:T(8,128)(2,1)S(1)} %pad_maximum_fusion.own_ref, bf16[16,64,1024]{2,1,0:T(8,128)(2,1)} %collective-permute-done.7.sib_ref), custom_call_target="tpu_custom_call" | custom-call | flops 536870912 | bytes 5242880 | tf_op jit(solution)/shard_map/pallas_call | solution.py:182
  132.2 0.0 collective-permute-done.9.sib_ref
  132.2 16.0 %all-to-all-done.1.r_ref = bf16[16,64,128]{2,1,0:T(8,128)(2,1)S(1)} async-done(((bf16[16,64,128]{2,1,0:T(8,128)(2,1)}), bf16[16,64,128]{2,1,0:T(8,128)(2,1)S(1)}, u32[]{:S(2)}, u32[]{:S(2)}) %all-to-all-start.1) | async-done | bytes 262176 | tf_op jit(solution)/shard_map/all_to_all | solution.py:239
  148.1 4.6 %shard_map.77 = bf16[1,128,2048]{2,1,0:T(8,128)(2,1)} custom-call(s32[1]{0:T(128)} %bitcast.pos_ref, bf16[16,64,128]{2,1,0:T(8,128)(2,1)S(1)} %all-to-all-done.1.r_ref, f32[128,1024]{1,0:T(8,128)S(1)} %shard_map.76.g_ref, bf16[16,64,1024]{2,1,0:T(8,128)(2,1)} %pad_maximum_fusion.1.own_ref, bf16[16,64,1024]{2,1,0:T(8,128)(2,1)} %collective-permute-done.9.sib_ref), custom_call_target="tpu_custom_call" | custom-call | flops 536870912 | bytes 6291456 | tf_op jit(solution)/shard_map/pallas_call | solution.py:192
  (1 shorter events, 0.0 us)
Async XLA Ops:
  46.4 22.2 %copy-start.1 = (bf16[128,1024]{1,0:T(8,128)(2,1)S(1)}, bf16[128,1024]{1,0:T(8,128)(2,1)}, u32[]{:S(2)}) copy-start(bf16[128,1024]{1,0:T(8,128)(2,1)} %shard_map.75) | copy-start | bytes 786436
  46.4 22.2 %collective-permute-start.3 = (bf16[128,1024]{1,0:T(8,128)(2,1)}, bf16[128,1024]{1,0:T(8,128)(2,1)S(1)}, u32[]{:S(2)}, u32[]{:S(2)}) collective-permute-start(bf16[128,1024]{1,0:T(8,128)(2,1)} %shard_map.75), channel_id=1, source_target_pairs={{0,6},{1,25},{2,0},{3,27},{4,2},{5,29},{6,4},{7,31},{8,14},{9,1},{... | collective-permute-start | bytes 786440 | tf_op jit(solution)/shard_map/ppermute | solution.py:215
  49.3 19.4 %collective-permute-start = (bf16[128,1024]{1,0:T(8,128)(2,1)}, bf16[128,1024]{1,0:T(8,128)(2,1)S(1)}, u32[]{:S(2)}, u32[]{:S(2)}) collective-permute-start(bf16[128,1024]{1,0:T(8,128)(2,1)} %shard_map.75), channel_id=1, source_target_pairs={{0,2},{1,9},{2,4},{3,11},{4,6},{5,13},{6,0},{7,15},{8,10},{9,17},{... | collective-permute-start | bytes 786440 | tf_op jit(solution)/shard_map/ppermute | solution.py:214
  54.6 14.0 %collective-permute-start.2 = (bf16[64,1024]{1,0:T(8,128)(2,1)S(1)}, bf16[64,1024]{1,0:T(8,128)(2,1)S(1)}, u32[]{:S(2)}, u32[]{:S(2)}) collective-permute-start(bf16[64,1024]{1,0:T(8,128)(2,1)S(1)} %get-tuple-element.20), channel_id=1, source_target_pairs={{0,4},{1,17},{2,6},{3,19},{4,0},{5,21},{6,2},{7,23},{8,12},{9,25},... | collective-permute-start | bytes 393224 | tf_op jit(solution)/shard_map/ppermute | solution.py:217
  56.7 11.9 %collective-permute-start.1 = (bf16[64,1024]{1,0:T(8,128)(2,1)S(1)}, bf16[64,1024]{1,0:T(8,128)(2,1)S(1)}, u32[]{:S(2)}, u32[]{:S(2)}) collective-permute-start(bf16[64,1024]{1,0:T(8,128)(2,1)S(1)} %get-tuple-element.19), channel_id=1, source_target_pairs={{0,4},{1,17},{2,6},{3,19},{4,0},{5,21},{6,2},{7,23},{8,12},{9,25},... | collective-permute-start | bytes 393224 | tf_op jit(solution)/shard_map/ppermute | solution.py:216
  62.0 47.2 %all-to-all-start = ((bf16[16,200,128]{2,1,0:T(8,128)(2,1)}), bf16[16,200,128]{2,1,0:T(8,128)(2,1)S(1)}, u32[]{:S(2)}, u32[]{:S(2)}) async-start(bf16[16,200,128]{2,1,0:T(8,128)(2,1)} %shard_map.73), calls=%async_computation | async-start | bytes 1638400 | tf_op jit(solution)/shard_map/all_to_all | solution.py:227
  68.8 28.5 %collective-permute-start.6 = (bf16[4,128,1024]{2,1,0:T(8,128)(2,1)S(1)}, bf16[4,128,1024]{2,1,0:T(8,128)(2,1)S(1)}, u32[]{:S(2)}, u32[]{:S(2)}) collective-permute-start(bf16[4,128,1024]{2,1,0:T(8,128)(2,1)S(1)} %pad_maximum_fusion.2), channel_id=1, source_target_pairs={{0,24},{1,7},{2,26},{3,1},{4,28},{5,3},{6,30},{7,5},{8,0},{9,15},{... | collective-permute-start | bytes 3145736 | tf_op jit(solution)/shard_map/ppermute | solution.py:215
  73.7 29.1 %collective-permute-start.4 = (bf16[4,128,1024]{2,1,0:T(8,128)(2,1)S(1)}, bf16[4,128,1024]{2,1,0:T(8,128)(2,1)S(1)}, u32[]{:S(2)}, u32[]{:S(2)}) collective-permute-start(bf16[4,128,1024]{2,1,0:T(8,128)(2,1)S(1)} %pad_maximum_fusion.2), channel_id=1, source_target_pairs={{0,8},{1,3},{2,10},{3,5},{4,12},{5,7},{6,14},{7,1},{8,16},{9,11},{... | collective-permute-start | bytes 3145736 | tf_op jit(solution)/shard_map/ppermute | solution.py:214
  75.8 27.2 %collective-permute-start.5 = (bf16[4,64,1024]{2,1,0:T(8,128)(2,1)S(1)}, bf16[4,64,1024]{2,1,0:T(8,128)(2,1)S(1)}, u32[]{:S(2)}, u32[]{:S(2)}) collective-permute-start(bf16[4,64,1024]{2,1,0:T(8,128)(2,1)S(1)} %get-tuple-element.16), channel_id=1, source_target_pairs={{0,16},{1,5},{2,18},{3,7},{4,20},{5,1},{6,22},{7,3},{8,24},{9,13},... | collective-permute-start | bytes 1572872 | tf_op jit(solution)/shard_map/ppermute | solution.py:216
  79.9 25.3 %collective-permute-start.8 = (bf16[4,64,1024]{2,1,0:T(8,128)(2,1)S(1)}, bf16[4,64,1024]{2,1,0:T(8,128)(2,1)S(1)}, u32[]{:S(2)}, u32[]{:S(2)}) collective-permute-start(bf16[4,64,1024]{2,1,0:T(8,128)(2,1)S(1)} %get-tuple-element.15), channel_id=1, source_target_pairs={{0,16},{1,5},{2,18},{3,7},{4,20},{5,1},{6,22},{7,3},{8,24},{9,13},... | collective-permute-start | bytes 1572872 | tf_op jit(solution)/shard_map/ppermute | solution.py:217
  103.3 26.5 %collective-permute-start.7 = (bf16[16,64,1024]{2,1,0:T(8,128)(2,1)S(1)}, bf16[16,64,1024]{2,1,0:T(8,128)(2,1)}, u32[]{:S(2)}, u32[]{:S(2)}) collective-permute-start(bf16[16,64,1024]{2,1,0:T(8,128)(2,1)S(1)} %pad_maximum_fusion.own_ref), channel_id=1, source_target_pairs={{0,1},{1,0},{2,3},{3,2},{4,5},{5,4},{6,7},{7,6},{8,9},{9,8},{10,11... | collective-permute-start | bytes 6291464 | tf_op jit(solution)/shard_map/ppermute | solution.py:235
  105.2 24.6 %copy-start = (bf16[1,128,2048]{2,1,0:T(8,128)(2,1)S(1)}, bf16[1,128,2048]{2,1,0:T(8,128)(2,1)}, u32[]{:S(2)}) copy-start(bf16[1,128,2048]{2,1,0:T(8,128)(2,1)} %h_ref.1) | copy-start | bytes 1572868
  106.8 25.4 %collective-permute-start.9 = (bf16[16,64,1024]{2,1,0:T(8,128)(2,1)}, bf16[16,64,1024]{2,1,0:T(8,128)(2,1)}, u32[]{:S(2)}, u32[]{:S(2)}) collective-permute-start(bf16[16,64,1024]{2,1,0:T(8,128)(2,1)} %pad_maximum_fusion.1.own_ref), channel_id=1, source_target_pairs={{0,1},{1,0},{2,3},{3,2},{4,5},{5,4},{6,7},{7,6},{8,9},{9,8},{10,11... | collective-permute-start | bytes 6291464 | tf_op jit(solution)/shard_map/ppermute | solution.py:236
  117.7 30.4 %all-to-all-start.1 = ((bf16[16,64,128]{2,1,0:T(8,128)(2,1)}), bf16[16,64,128]{2,1,0:T(8,128)(2,1)S(1)}, u32[]{:S(2)}, u32[]{:S(2)}) async-start(bf16[16,64,128]{2,1,0:T(8,128)(2,1)} %shard_map.74), calls=%async_computation.1 | async-start | bytes 524288 | tf_op jit(solution)/shard_map/all_to_all | solution.py:239

commit v3 on v1

--- a/solution.py
+++ b/solution.py
@@ -5,6 +5,7 @@
 from jax.experimental import pallas as pl
 from jax.experimental.pallas import tpu as pltpu
 from jax.sharding import PartitionSpec as P
+
 
 eps_norm = 1e-05
 log2e = math.log2(math.e)
@@ -131,22 +132,23 @@
     )(buf)
 
 
-def gate_kernel(h_ref, w_ref, out_ref, acc_ref):
+def gate_kernel(h_ref, w_ref, out_ref, o_ref):
     j = pl.program_id(0)
-    w = w_ref[:, 0].reshape(256, 1024)
-    part = mm(h_ref[0], w)
+    first = jnp.concatenate([w_ref[i, :, 0:64] for i in range(4)], axis=1)
+    o_ref[:, pl.ds(pl.multiple_of(256 * j, 256), 256)] = jnp.concatenate([w_ref[i, :, 64:128] for i in range(4)], axis=1)
+    part = mm(h_ref[0], first, 1, 1)
 
     @pl.when(j == 0)
     def _():
-        acc_ref[...] = part
+        out_ref[...] = part
 
     @pl.when(j > 0)
     def _():
-        acc_ref[...] += part
+        out_ref[...] += part
 
     @pl.when(j == pl.num_programs(0) - 1)
     def _():
-        v = acc_ref[...]
+        v = out_ref[...]
         out_ref[...] = v / (1.0 + jnp.exp(-v))
 
 
@@ -156,63 +158,53 @@
         grid=(8,),
         in_specs=[
             pl.BlockSpec((1, TOK, 256), lambda j: (0, 0, j)),
-            pl.BlockSpec((4, 1, 64, 1024), lambda j: (j, 0, 0, 0)),
+            pl.BlockSpec((4, 1024, 128), lambda j: (j, 0, 0)),
         ],
-        out_specs=pl.BlockSpec((TOK, 1024), lambda j: (0, 0)),
-        out_shape=jax.ShapeDtypeStruct((TOK, 1024), f32),
-        scratch_shapes=[pltpu.VMEM((TOK, 1024), f32)],
-        cost_estimate=pl.CostEstimate(flops=2 * 128 * 1024 * 2048, bytes_accessed=5 << 20, transcendentals=1 << 17),
+        out_specs=[
+            pl.BlockSpec((TOK, 1024), lambda j: (0, 0)),
+            pl.BlockSpec((1024, 2048), lambda j: (0, 0)),
+        ],
+        out_shape=[jax.ShapeDtypeStruct((TOK, 1024), f32), jax.ShapeDtypeStruct((1024, 2048), bf16)],
+        compiler_params=pltpu.CompilerParams(vmem_limit_bytes=32 * 1024 * 1024),
+        cost_estimate=pl.CostEstimate(flops=2 * 128 * 1024 * 2048, bytes_accessed=12 << 20, transcendentals=1 << 17),
     )(hidden, w)
 
 
-def mix_kernel(r_ref, g_ref, w_ref, out_ref, gd_ref):
-    @pl.when(pl.program_id(0) == 0)
-    def _():
-        for h in range(0, SRC, 2):
-            a, b = r_ref[h], r_ref[h + 1]
-            top = jnp.concatenate([a[:, 0:HD], b[:, 0:HD]], axis=1)
-            bot = jnp.concatenate([a[:, HD:], b[:, HD:]], axis=1)
-            n = jnp.concatenate([top, bot], axis=0).astype(f32)
-            s = slice(HD * h, HD * h + 2 * HD)
-            gd_ref[:, s] = (n * g_ref[:, s]).astype(bf16)
-
-    w = w_ref[:, 0].reshape(256, 1024)
-    out_ref[0] = mm(gd_ref[...], w, 1, 1).astype(bf16)
-
-
-def mix(ret, gact, w):
+def mix_kernel(r_ref, g_ref, o_ref, out_ref, gd_ref):
+    for h in range(0, SRC, 2):
+        a, b = r_ref[h], r_ref[h + 1]
+        top = jnp.concatenate([a[:, 0:HD], b[:, 0:HD]], axis=1)
+        bot = jnp.concatenate([a[:, HD:], b[:, HD:]], axis=1)
+        n = jnp.concatenate([top, bot], axis=0).astype(f32)
+        s = slice(HD * h, HD * h + 2 * HD)
+        gd_ref[:, s] = (n * g_ref[:, s]).astype(bf16)
+    for j in range(4):
+        s = slice(512 * j, 512 * j + 512)
+        out_ref[0, :, s] = mm(gd_ref[...], o_ref[:, s]).astype(bf16)
+
+
+def mix(ret, gact, o):
     return pl.pallas_call(
         mix_kernel,
-        grid=(8,),
-        in_specs=[
-            pl.BlockSpec((SRC, 64, TOK), lambda j: (0, 0, 0)),
-            pl.BlockSpec((TOK, 1024), lambda j: (0, 0)),
-            pl.BlockSpec((4, 1, 64, 1024), lambda j: (j, 1, 0, 0)),
-        ],
-        out_specs=pl.BlockSpec((1, TOK, 256), lambda j: (0, 0, j)),
         out_shape=jax.ShapeDtypeStruct((1, TOK, 2048), bf16),
         scratch_shapes=[pltpu.VMEM((TOK, 1024), bf16)],
+        compiler_params=pltpu.CompilerParams(vmem_limit_bytes=32 * 1024 * 1024),
         cost_estimate=pl.CostEstimate(flops=2 * 128 * 1024 * 2048, bytes_accessed=6 << 20, transcendentals=0),
-    )(ret, gact, w)
-
-
-def turn_kernel(x_ref, out_ref):
-    out_ref[...] = x_ref[...].T
-
-
-def turn(x):
-    return pl.pallas_call(turn_kernel, out_shape=jax.ShapeDtypeStruct((128, 1024), bf16))(x)
+    )(ret, gact, o)
 
 
 def shards(queries, key_rows, value_rows, break_offset, hidden_in, gate_weight, out_weight):
-    own = jnp.concatenate([gate_weight.T, out_weight], axis=1)
-    cols = turn(lax.all_gather(own, "sp", axis=0, tiled=True))
-    w = lax.all_gather(cols[None], "dp", axis=0, tiled=True).reshape(32, 2, 64, 1024)
+    joined = jnp.concatenate([gate_weight.T, out_weight], axis=1)
+    joined = jnp.broadcast_to(joined[None], (SRC, 64, TOK))
+    joined = lax.all_to_all(joined, "sp", split_axis=0, concat_axis=0, tiled=True)
     buf = pack(queries, key_rows, value_rows, break_offset)
+    buf, joined = lax.optimization_barrier((buf, joined))
+    w = lax.all_gather(joined.reshape(1, 1024, TOK), "dp", axis=0, tiled=True)
     buf = lax.all_to_all(buf, "sp", split_axis=0, concat_axis=0, tiled=True)
     heads = attend(buf)
     ret = lax.all_to_all(heads, "sp", split_axis=0, concat_axis=0, tiled=True)
-    return mix(ret, gate(hidden_in, w), w)
+    gact, o = gate(hidden_in, w)
+    return mix(ret, gact, o)
 
 
 def solution(mesh):

time: 141 us -> 135 us (0.957)
  the two profiles are of different devices: /device:TPU:30 before, /device:TPU:4 now
where the time goes in v3:
time: 135 us; the launch traced here: 134 us
  blocking collectives  48.3 us (36%)
  waiting for transfers between devices  22.5 us (17%)
  starting transfers between devices  20.6 us (15%)
  Pallas kernels  16.5 us (12%)
  between operations  13.4 us (10%)
  local copies, waits for them, and re-layouts  12.2 us (9%)
    all_to_all x1, blocking collectives, shards(): buf = lax.all_to_all(buf, 'sp', split_axis=0, concat_axis=0, tiled=True)  48.3 us
    all_to_all x1, starting transfers between devices, shards(): lax.all_to_all(joined, 'sp', split_axis=0, concat_axis=0, tiled=True)  15.2 us
    all_to_all x1, waiting for transfers between devices, shards(): lax.all_to_all(joined, 'sp', split_axis=0, concat_axis=0, tiled=True)  14.5 us
    unnamed x12, local copies, waits for them, and re-layouts  11.5 us
    pallas_call x1, Pallas kernels, attend(): pl.pallas_call(attn_kernel, out_shape=jax.ShapeDtypeStruct((SRC, 64, TOK)...  8.52 us
    all_to_all x1, waiting for transfers between devices, shards(): ret = lax.all_to_all(heads, 'sp', split_axis=0, concat_axis=0, tiled=True)  7.16 us
    all_to_all x1, starting transfers between devices, shards(): ret = lax.all_to_all(heads, 'sp', split_axis=0, concat_axis=0, tiled=True)  5.4 us
    pallas_call x1, Pallas kernels, gate(): pl.pallas_call(gate_kernel, grid=(8,), in_specs=[pl.BlockSpec((1, TOK, 25...  3.94 us
  transfers between devices with their start and end apart: 3, of which 3 were waited for; matrix products, arithmetic and copies ran while one was open for 1% of the time, Pallas kernels for 11%

profile of v3, /device:TPU:4, one launch (start us, length us, event | category | flops | bytes accessed | tf_op | source)
XLA Modules:
  0.0 134.5 jit_solution(11364835246747962274)
XLA Ops:
  6.5 0.8 copy.11
  7.3 0.8 pad_maximum_fusion
  8.1 0.8 broadcast_in_dim.2
  8.9 15.2 %all-to-all-start = ((bf16[16,64,128]{2,1,0:T(8,128)(2,1)}), bf16[16,64,128]{2,1,0:T(8,128)(2,1)S(1)}, u32[]{:S(2)}, u32[]{:S(2)}) async-start(bf16[16,64,128]{2,1,0:T(8,128)(2,1)} %broadcast_in_dim.2), calls=%async_computation | async-start | bytes 524288 | tf_op jit(solution)/shard_map/all_to_all | solution.py:199
  24.1 0.0 all-gather.2.cloned.1.call-start
  24.2 1.4 %copy.10.o_ref = bf16[1,128,16]{2,1,0:T(8,128)(2,1)} copy(bf16[1,128,16]{1,2,0:T(8,128)(2,1)} %param.10) | data formatting | bytes 8192 | tf_op args[3]
  25.6 2.5 %shard_map.73 = bf16[16,200,128]{2,1,0:T(8,128)(2,1)} custom-call(bf16[1,128,1024]{2,1,0:T(8,128)(2,1)} %q_ref.1, bf16[1,128,1024]{2,1,0:T(8,128)(2,1)} %k_ref.1, bf16[1,128,1024]{2,1,0:T(8,128)(2,1)} %v_ref.1, bf16[1,128,16]{2,1,0:T(8,128)(2,1)} %copy.10.o_ref), custom_call_target="tpu_custom_call" | custom-call | tf_op jit(solution)/shard_map/pallas_call | solution.py:37
  28.0 14.5 %all-to-all-done = bf16[16,64,128]{2,1,0:T(8,128)(2,1)S(1)} async-done(((bf16[16,64,128]{2,1,0:T(8,128)(2,1)}), bf16[16,64,128]{2,1,0:T(8,128)(2,1)S(1)}, u32[]{:S(2)}, u32[]{:S(2)}) %all-to-all-start) | async-done | bytes 262176 | tf_op jit(solution)/shard_map/all_to_all | solution.py:199
  42.5 0.0 copy-start.4
  42.5 0.7 copy-done.4
  43.2 0.0 all-gather.2.cloned.1.call-update
  43.2 48.3 %all_to_all.15.buf_ref = bf16[16,200,128]{2,1,0:T(8,128)(2,1)S(1)} all-to-all(bf16[16,200,128]{2,1,0:T(8,128)(2,1)} %shard_map.73), channel_id=1, replica_groups=mesh['sp'=16,'dp'=32] {'sp'}, dimensions={0} | all-to-all | bytes 1638400 | tf_op jit(solution)/shard_map/all_to_all | solution.py:203
  91.6 8.5 %shard_map.74 = bf16[16,64,128]{2,1,0:T(8,128)(2,1)} custom-call(bf16[16,200,128]{2,1,0:T(8,128)(2,1)S(1)} %all_to_all.15.buf_ref), custom_call_target="tpu_custom_call" | custom-call | tf_op jit(solution)/shard_map/pallas_call | solution.py:122
  100.1 5.4 %all-to-all-start.2 = ((bf16[16,64,128]{2,1,0:T(8,128)(2,1)}), bf16[16,64,128]{2,1,0:T(8,128)(2,1)S(1)}, u32[]{:S(2)}, u32[]{:S(2)}) async-start(bf16[16,64,128]{2,1,0:T(8,128)(2,1)} %shard_map.74), calls=%async_computation.2 | async-start | bytes 524288 | tf_op jit(solution)/shard_map/all_to_all | solution.py:205
  105.5 0.9 all-gather.2.cloned.1.call-done.w_ref
  106.4 0.0 copy-start
  106.4 3.4 %copy-done = bf16[32,1024,128]{2,1,0:T(8,128)(2,1)S(1)} copy-done((bf16[32,1024,128]{2,1,0:T(8,128)(2,1)S(1)}, bf16[32,1024,128]{2,1,0:T(8,128)(2,1)}, u32[]{:S(2)}) %copy-start) | copy-done | bytes 8388632
  109.8 0.0 copy-start.3
  109.8 1.0 copy-done.3
  110.8 3.9 %shard_map.75 = (f32[128,1024]{1,0:T(8,128)S(1)}, bf16[1024,2048]{1,0:T(8,128)(2,1)S(1)}) custom-call(bf16[1,128,2048]{2,1,0:T(8,128)(2,1)S(1)} %copy-done.3, bf16[32,1024,128]{2,1,0:T(8,128)(2,1)S(1)} %copy-done), custom_call_target="tpu_custom_call" | custom-call | flops 536870912 | bytes 12582912 | tf_op jit(solution)/shard_map/pallas_call | solution.py:156
  114.7 0.0 copy-start.1
  114.8 1.9 %copy-done.1 = bf16[1024,2048]{1,0:T(8,128)(2,1)} copy-done((bf16[1024,2048]{1,0:T(8,128)(2,1)}, bf16[1024,2048]{1,0:T(8,128)(2,1)S(1)}, u32[]{:S(2)}) %copy-start.1) | copy-done | bytes 4194328
  116.7 7.2 %all-to-all-done.2.r_ref = bf16[16,64,128]{2,1,0:T(8,128)(2,1)S(1)} async-done(((bf16[16,64,128]{2,1,0:T(8,128)(2,1)}), bf16[16,64,128]{2,1,0:T(8,128)(2,1)S(1)}, u32[]{:S(2)}, u32[]{:S(2)}) %all-to-all-start.2) | async-done | bytes 262176 | tf_op jit(solution)/shard_map/all_to_all | solution.py:205
  123.9 0.0 copy-start.2
  123.9 2.2 %copy-done.2 = bf16[1024,2048]{1,0:T(8,128)(2,1)S(1)} copy-done((bf16[1024,2048]{1,0:T(8,128)(2,1)S(1)}, bf16[1024,2048]{1,0:T(8,128)(2,1)}, u32[]{:S(2)}) %copy-start.2) | copy-done | bytes 4194328
  126.1 1.6 %shard_map.76 = bf16[1,128,2048]{2,1,0:T(8,128)(2,1)} custom-call(bf16[16,64,128]{2,1,0:T(8,128)(2,1)S(1)} %all-to-all-done.2.r_ref, f32[128,1024]{1,0:T(8,128)S(1)} %get-tuple-element.11.g_ref, bf16[1024,2048]{1,0:T(8,128)(2,1)S(1)} %copy-done.2), custom_call_target="tpu_custom_call" | custom-call | flops 536870912 | bytes 6291456 | tf_op jit(solution)/shard_map/pallas_call | solution.py:187
Async XLA Ops:
  8.9 33.6 %all-to-all-start = ((bf16[16,64,128]{2,1,0:T(8,128)(2,1)}), bf16[16,64,128]{2,1,0:T(8,128)(2,1)S(1)}, u32[]{:S(2)}, u32[]{:S(2)}) async-start(bf16[16,64,128]{2,1,0:T(8,128)(2,1)} %broadcast_in_dim.2), calls=%async_computation | async-start | bytes 524288 | tf_op jit(solution)/shard_map/all_to_all | solution.py:199
  24.1 82.3 %all-gather.2.cloned.1.call-start = ((), (), s32[]{:S(2)}) async-start(), calls=%async_computation.3 | async-start | bytes 8650752 | tf_op jit(solution)/shard_map/all_gather | solution.py:202
  42.5 0.7 copy-start.4
  100.1 23.8 %all-to-all-start.2 = ((bf16[16,64,128]{2,1,0:T(8,128)(2,1)}), bf16[16,64,128]{2,1,0:T(8,128)(2,1)S(1)}, u32[]{:S(2)}, u32[]{:S(2)}) async-start(bf16[16,64,128]{2,1,0:T(8,128)(2,1)} %shard_map.74), calls=%async_computation.2 | async-start | bytes 524288 | tf_op jit(solution)/shard_map/all_to_all | solution.py:205
  106.4 3.4 %copy-start = (bf16[32,1024,128]{2,1,0:T(8,128)(2,1)S(1)}, bf16[32,1024,128]{2,1,0:T(8,128)(2,1)}, u32[]{:S(2)}) copy-start(bf16[32,1024,128]{2,1,0:T(8,128)(2,1)} %all-gather.2.cloned.1.call-done.w_ref) | copy-start | bytes 25165828
  109.8 1.0 copy-start.3
  114.7 2.0 %copy-start.1 = (bf16[1024,2048]{1,0:T(8,128)(2,1)}, bf16[1024,2048]{1,0:T(8,128)(2,1)S(1)}, u32[]{:S(2)}) copy-start(bf16[1024,2048]{1,0:T(8,128)(2,1)S(1)} %get-tuple-element.12.o_ref) | copy-start | bytes 12582916
  123.9 2.2 %copy-start.2 = (bf16[1024,2048]{1,0:T(8,128)(2,1)S(1)}, bf16[1024,2048]{1,0:T(8,128)(2,1)}, u32[]{:S(2)}) copy-start(bf16[1024,2048]{1,0:T(8,128)(2,1)} %copy-done.1) | copy-start | bytes 12582916
Sparse Core Ops, SparseCore 0:
  43.3 62.9 all-gather.1

commit v4 on v3

--- a/solution.py
+++ b/solution.py
@@ -19,13 +19,15 @@
     return lax.dot_general(a, b, (((ca,), (cb,)), ((), ())), preferred_element_type=f32)
 
 
-def pack_kernel(q_ref, k_ref, v_ref, o_ref, out_ref):
+def pack_kernel(q_ref, k_ref, v_ref, o_ref, gw_ref, ow_ref, out_ref, joined_ref):
     row = lax.broadcasted_iota(jnp.int32, (TOK, TOK), 0)
     col = lax.broadcasted_iota(jnp.int32, (TOK, TOK), 1)
     perm = jnp.where(col == GRP * (row % 32) + row // 32, 1.0, 0.0).astype(bf16)
     keys = mm(perm, k_ref[0]).astype(bf16)
     vals = mm(perm, v_ref[0]).astype(bf16)
-    offs = mm(o_ref[0], perm, 0, 1).astype(bf16)
+    offs = mm(o_ref[0], perm, 1, 1).astype(bf16)
+    eye = jnp.where(row[0:HD, 0:HD] == col[0:HD, 0:HD], 1.0, 0.0).astype(bf16)
+    joined_ref[...] = jnp.concatenate([mm(gw_ref[...], eye, 0, 0).astype(bf16), ow_ref[...]], axis=1)
     for h in range(SRC):
         s = slice(HD * h, HD * h + HD)
         out_ref[h, 0:TOK, :] = jnp.concatenate([q_ref[0, :, s], keys[:, s]], axis=1)
@@ -33,11 +35,11 @@
         out_ref[h, 192:200, :] = jnp.broadcast_to(offs[h : h + 1, :], (8, TOK))
 
 
-def pack(q, k, v, o):
+def pack(q, k, v, o, gw, ow):
     return pl.pallas_call(
         pack_kernel,
-        out_shape=jax.ShapeDtypeStruct((SRC, ROWS, TOK), bf16),
-    )(q, k, v, o)
+        out_shape=[jax.ShapeDtypeStruct((SRC, ROWS, TOK), bf16), jax.ShapeDtypeStruct((HD, TOK), bf16)],
+    )(q, k, v, o.transpose(0, 2, 1), gw, ow)
 
 
 def attn_kernel(buf_ref, out_ref, qq, kk, vv, of):
@@ -66,7 +68,7 @@
     tc = lax.broadcasted_iota(jnp.int32, (256, 256), 1)
     tri = jnp.where((tc >= TOK) | (tr > tc), -1.0, 0.0).astype(bf16)
 
-    R = 256
+    R = 512
 
     def block(qt, b, qrow, carry, acc, diag):
         ks = b * 512
@@ -135,7 +137,7 @@
 def gate_kernel(h_ref, w_ref, out_ref, o_ref):
     j = pl.program_id(0)
     first = jnp.concatenate([w_ref[i, :, 0:64] for i in range(4)], axis=1)
-    o_ref[:, pl.ds(pl.multiple_of(256 * j, 256), 256)] = jnp.concatenate([w_ref[i, :, 64:128] for i in range(4)], axis=1)
+    o_ref[...] = jnp.concatenate([w_ref[i, :, 64:128] for i in range(4)], axis=1)
     part = mm(h_ref[0], first, 1, 1)
 
     @pl.when(j == 0)
@@ -162,7 +164,7 @@
         ],
         out_specs=[
             pl.BlockSpec((TOK, 1024), lambda j: (0, 0)),
-            pl.BlockSpec((1024, 2048), lambda j: (0, 0)),
+            pl.BlockSpec((1024, 256), lambda j: (0, j)),
         ],
         out_shape=[jax.ShapeDtypeStruct((TOK, 1024), f32), jax.ShapeDtypeStruct((1024, 2048), bf16)],
         compiler_params=pltpu.CompilerParams(vmem_limit_bytes=32 * 1024 * 1024),
@@ -170,7 +172,12 @@
     )(hidden, w)
 
 
-def mix_kernel(r_ref, g_ref, o_ref, out_ref, gd_ref):
+def mix_kernel(r_ref, g_ref, o_ref, out_ref, gd_ref, ow_ref, sems):
+    copies = [
+        pltpu.make_async_copy(o_ref.at[:, 512 * j : 512 * j + 512], ow_ref.at[j], sems.at[j]) for j in range(4)
+    ]
+    for c in copies:
+        c.start()
     for h in range(0, SRC, 2):
         a, b = r_ref[h], r_ref[h + 1]
         top = jnp.concatenate([a[:, 0:HD], b[:, 0:HD]], axis=1)
@@ -179,25 +186,32 @@
         s = slice(HD * h, HD * h + 2 * HD)
         gd_ref[:, s] = (n * g_ref[:, s]).astype(bf16)
     for j in range(4):
-        s = slice(512 * j, 512 * j + 512)
-        out_ref[0, :, s] = mm(gd_ref[...], o_ref[:, s]).astype(bf16)
+        copies[j].wait()
+        out_ref[0, :, 512 * j : 512 * j + 512] = mm(gd_ref[...], ow_ref[j]).astype(bf16)
 
 
 def mix(ret, gact, o):
     return pl.pallas_call(
         mix_kernel,
+        in_specs=[
+            pl.BlockSpec(memory_space=pltpu.VMEM),
+            pl.BlockSpec(memory_space=pltpu.VMEM),
+            pl.BlockSpec(memory_space=pltpu.HBM),
+        ],
         out_shape=jax.ShapeDtypeStruct((1, TOK, 2048), bf16),
-        scratch_shapes=[pltpu.VMEM((TOK, 1024), bf16)],
-        compiler_params=pltpu.CompilerParams(vmem_limit_bytes=32 * 1024 * 1024),
+        scratch_shapes=[
+            pltpu.VMEM((TOK, 1024), bf16),
+            pltpu.VMEM((4, 1024, 512), bf16),
+            pltpu.SemaphoreType.DMA((4,)),
+        ],
+        compiler_params=pltpu.CompilerParams(vmem_limit_bytes=16 * 1024 * 1024),
         cost_estimate=pl.CostEstimate(flops=2 * 128 * 1024 * 2048, bytes_accessed=6 << 20, transcendentals=0),
-    )(ret, gact, o)
+    )(ret, gact, pltpu.with_memory_space_constraint(o, pltpu.HBM))
 
 
 def shards(queries, key_rows, value_rows, break_offset, hidden_in, gate_weight, out_weight):
-    joined = jnp.concatenate([gate_weight.T, out_weight], axis=1)
-    joined = jnp.broadcast_to(joined[None], (SRC, 64, TOK))
-    joined = lax.all_to_all(joined, "sp", split_axis=0, concat_axis=0, tiled=True)
-    buf = pack(queries, key_rows, value_rows, break_offset)
+    buf, joined = pack(queries, key_rows, value_rows, break_offset, gate_weight, out_weight)
+    joined = lax.all_gather(joined, "sp", axis=0, tiled=True)
     buf, joined = lax.optimization_barrier((buf, joined))
     w = lax.all_gather(joined.reshape(1, 1024, TOK), "dp", axis=0, tiled=True)
     buf = lax.all_to_all(buf, "sp", split_axis=0, concat_axis=0, tiled=True)

time: 135 us -> 135 us (level)
  the two profiles are of different devices: /device:TPU:4 before, /device:TPU:1 now
where the time goes in v4:
time: 135 us
  blocking collectives  70.1 us (52%)
  Pallas kernels  16.2 us (12%)
  waiting for transfers between devices  15 us (11%)
  starting transfers between devices  13.6 us (10%)
  between operations  13.4 us (10%)
  local copies, waits for them, and re-layouts  6.36 us (5%)
    all_to_all x1, blocking collectives, shards(): buf = lax.all_to_all(buf, 'sp', split_axis=0, concat_axis=0, tiled=True)  36.8 us
    all_gather x1, blocking collectives, shards(): joined = lax.all_gather(joined, 'sp', axis=0, tiled=True)  33.3 us
    all_gather x1, waiting for transfers between devices, shards(): w = lax.all_gather(joined.reshape(1, 1024, TOK), 'dp', axis=0, tiled=True)  14.9 us
    all_to_all x1, starting transfers between devices, shards(): ret = lax.all_to_all(heads, 'sp', split_axis=0, concat_axis=0, tiled=True)  13.6 us
    unnamed x6, local copies, waits for them, and re-layouts  6.36 us
    pallas_call x1, Pallas kernels, attend(): pl.pallas_call(attn_kernel, out_shape=jax.ShapeDtypeStruct((SRC, 64, TOK)...  6.03 us
    pallas_call x1, Pallas kernels, gate(): pl.pallas_call(gate_kernel, grid=(8,), in_specs=[pl.BlockSpec((1, TOK, 25...  4.32 us
    pallas_call x1, Pallas kernels, mix(): pl.pallas_call(mix_kernel, in_specs=[pl.BlockSpec(memory_space=pltpu.VMEM...  3.39 us
  transfers between devices with their start and end apart: 2, of which 1 were waited for; matrix products, arithmetic and copies ran while one was open for 0% of the time, Pallas kernels for 8%

profile of v4, /device:TPU:1, one launch (start us, length us, event | category | flops | bytes accessed | tf_op | source)
XLA Modules:
  0.0 134.7 jit_solution(12266473129283087733)
XLA Ops:
  6.5 0.0 all-gather.3.cloned.1.call-start
  6.5 2.5 %shard_map.73 = (bf16[16,200,128]{2,1,0:T(8,128)(2,1)}, bf16[64,128]{1,0:T(8,128)(2,1)}) custom-call(bf16[1,128,1024]{2,1,0:T(8,128)(2,1)} %q_ref.1, bf16[1,128,1024]{2,1,0:T(8,128)(2,1)} %k_ref.1, bf16[1,128,1024]{2,1,0:T(8,128)(2,1)} %v_ref.1, bf16[1,16,128]{2,1,0:T(8,128)(2,1)} %bitcast.3, bf16[64,64]{1,0:T(8,128)(2,1)} %gw_ref.1, bf16[64,64]{1,0:T(8,128)(2,1)} %ow_ref.1), custom_call_target="tpu_custom_call" | custom-call | tf_op jit(solution)/shard_map/pallas_call | solution.py:39
  9.0 33.3 %all_gather.6 = bf16[1024,128]{1,0:T(8,128)(2,1)} all-gather(bf16[64,128]{1,0:T(8,128)(2,1)} %get-tuple-element.12), channel_id=1, replica_groups=mesh['sp'=16,'dp'=32] {'sp'}, dimensions={0}, use_global_device_ids=true | all-gather | bytes 278528 | tf_op jit(solution)/shard_map/all_gather | solution.py:214
  42.3 0.0 all-gather.3.cloned.1.call-update
  42.4 36.8 %all_to_all.10.buf_ref = bf16[16,200,128]{2,1,0:T(8,128)(2,1)S(1)} all-to-all(bf16[16,200,128]{2,1,0:T(8,128)(2,1)} %get-tuple-element.13), channel_id=1, replica_groups=mesh['sp'=16,'dp'=32] {'sp'}, dimensions={0} | all-to-all | bytes 1638400 | tf_op jit(solution)/shard_map/all_to_all | solution.py:217
  79.1 6.0 %shard_map.74 = bf16[16,64,128]{2,1,0:T(8,128)(2,1)} custom-call(bf16[16,200,128]{2,1,0:T(8,128)(2,1)S(1)} %all_to_all.10.buf_ref), custom_call_target="tpu_custom_call" | custom-call | tf_op jit(solution)/shard_map/pallas_call | solution.py:124
  85.2 13.6 %all-to-all-start.1 = ((bf16[16,64,128]{2,1,0:T(8,128)(2,1)}), bf16[16,64,128]{2,1,0:T(8,128)(2,1)S(1)}, u32[]{:S(2)}, u32[]{:S(2)}) async-start(bf16[16,64,128]{2,1,0:T(8,128)(2,1)} %shard_map.74), calls=%async_computation.1 | async-start | bytes 524288 | tf_op jit(solution)/shard_map/all_to_all | solution.py:219
  98.8 14.9 %all-gather.3.cloned.1.call-done = bf16[32768,128]{1,0:T(8,128)(2,1)} async-done(((bf16[1024,128]{1,0:T(8,128)(2,1)}), bf16[32768,128]{1,0:T(8,128)(2,1)}) %all-gather.3.cloned.1.call-update) | async-done | bytes 8388624 | tf_op jit(solution)/shard_map/all_gather | solution.py:216
  113.8 0.0 copy-start
  113.8 3.4 %copy-done = bf16[32768,128]{1,0:T(8,128)(2,1)S(1)} copy-done((bf16[32768,128]{1,0:T(8,128)(2,1)S(1)}, bf16[32768,128]{1,0:T(8,128)(2,1)}, u32[]{:S(2)}) %copy-start) | copy-done | bytes 8388632
  117.1 0.0 copy-start.2
  117.1 1.0 copy-done.2
  118.2 4.3 %shard_map.75 = (f32[128,1024]{1,0:T(8,128)S(1)}, bf16[1024,2048]{1,0:T(8,128)(2,1)S(1)}) custom-call(bf16[1,128,2048]{2,1,0:T(8,128)(2,1)S(1)} %copy-done.2, bf16[32,1024,128]{2,1,0:T(8,128)(2,1)S(1)} %bitcast.2), custom_call_target="tpu_custom_call" | custom-call | flops 536870912 | bytes 12582912 | tf_op jit(solution)/shard_map/pallas_call | solution.py:158
  122.5 0.0 copy-start.1
  122.5 1.9 %copy-done.1 = bf16[1024,2048]{1,0:T(8,128)(2,1)} copy-done((bf16[1024,2048]{1,0:T(8,128)(2,1)}, bf16[1024,2048]{1,0:T(8,128)(2,1)S(1)}, u32[]{:S(2)}) %copy-start.1) | copy-done | bytes 4194328
  124.5 0.0 all-to-all-done.1.r_ref
  124.5 3.4 %shard_map.76 = bf16[1,128,2048]{2,1,0:T(8,128)(2,1)} custom-call(bf16[16,64,128]{2,1,0:T(8,128)(2,1)S(1)} %all-to-all-done.1.r_ref, f32[128,1024]{1,0:T(8,128)S(1)} %get-tuple-element.15.g_ref, bf16[1024,2048]{1,0:T(8,128)(2,1)} %copy-done.1), custom_call_target="tpu_custom_call" | custom-call | flops 536870912 | bytes 6291456 | tf_op jit(solution)/shard_map/pallas_call | solution.py:194
Async XLA Ops:
  6.5 107.2 %all-gather.3.cloned.1.call-start = ((), (), s32[]{:S(2)}) async-start(), calls=%async_computation.2 | async-start | bytes 8650752 | tf_op jit(solution)/shard_map/all_gather | solution.py:216
  85.2 39.3 %all-to-all-start.1 = ((bf16[16,64,128]{2,1,0:T(8,128)(2,1)}), bf16[16,64,128]{2,1,0:T(8,128)(2,1)S(1)}, u32[]{:S(2)}, u32[]{:S(2)}) async-start(bf16[16,64,128]{2,1,0:T(8,128)(2,1)} %shard_map.74), calls=%async_computation.1 | async-start | bytes 524288 | tf_op jit(solution)/shard_map/all_to_all | solution.py:219
  113.8 3.4 %copy-start = (bf16[32768,128]{1,0:T(8,128)(2,1)S(1)}, bf16[32768,128]{1,0:T(8,128)(2,1)}, u32[]{:S(2)}) copy-start(bf16[32768,128]{1,0:T(8,128)(2,1)} %all-gather.3.cloned.1.call-done) | copy-start | bytes 25165828
  117.1 1.0 copy-start.2
  122.5 1.9 %copy-start.1 = (bf16[1024,2048]{1,0:T(8,128)(2,1)}, bf16[1024,2048]{1,0:T(8,128)(2,1)S(1)}, u32[]{:S(2)}) copy-start(bf16[1024,2048]{1,0:T(8,128)(2,1)S(1)} %get-tuple-element.16.o_ref) | copy-start | bytes 12582916
Sparse Core Ops, SparseCore 0:
  42.5 71.2 all-gather.2

commit v5 on v4

--- a/solution.py
+++ b/solution.py
@@ -137,7 +137,7 @@
 def gate_kernel(h_ref, w_ref, out_ref, o_ref):
     j = pl.program_id(0)
     first = jnp.concatenate([w_ref[i, :, 0:64] for i in range(4)], axis=1)
-    o_ref[...] = jnp.concatenate([w_ref[i, :, 64:128] for i in range(4)], axis=1)
+    o_ref[0] = jnp.concatenate([w_ref[i, :, 64:128] for i in range(4)], axis=1)
     part = mm(h_ref[0], first, 1, 1)
 
     @pl.when(j == 0)
@@ -164,18 +164,16 @@
         ],
         out_specs=[
             pl.BlockSpec((TOK, 1024), lambda j: (0, 0)),
-            pl.BlockSpec((1024, 256), lambda j: (0, j)),
-        ],
-        out_shape=[jax.ShapeDtypeStruct((TOK, 1024), f32), jax.ShapeDtypeStruct((1024, 2048), bf16)],
+            pl.BlockSpec((1, 1024, 256), lambda j: (j, 0, 0)),
+        ],
+        out_shape=[jax.ShapeDtypeStruct((TOK, 1024), f32), pltpu.HBM((8, 1024, 256), bf16)],
         compiler_params=pltpu.CompilerParams(vmem_limit_bytes=32 * 1024 * 1024),
         cost_estimate=pl.CostEstimate(flops=2 * 128 * 1024 * 2048, bytes_accessed=12 << 20, transcendentals=1 << 17),
-    )(hidden, w)
+    )(pltpu.with_memory_space_constraint(hidden, pltpu.HBM), pltpu.with_memory_space_constraint(w, pltpu.HBM))
 
 
 def mix_kernel(r_ref, g_ref, o_ref, out_ref, gd_ref, ow_ref, sems):
-    copies = [
-        pltpu.make_async_copy(o_ref.at[:, 512 * j : 512 * j + 512], ow_ref.at[j], sems.at[j]) for j in range(4)
-    ]
+    copies = [pltpu.make_async_copy(o_ref.at[j], ow_ref.at[j], sems.at[j]) for j in range(8)]
     for c in copies:
         c.start()
     for h in range(0, SRC, 2):
@@ -185,9 +183,9 @@
         n = jnp.concatenate([top, bot], axis=0).astype(f32)
         s = slice(HD * h, HD * h + 2 * HD)
         gd_ref[:, s] = (n * g_ref[:, s]).astype(bf16)
-    for j in range(4):
+    for j in range(8):
         copies[j].wait()
-        out_ref[0, :, 512 * j : 512 * j + 512] = mm(gd_ref[...], ow_ref[j]).astype(bf16)
+        out_ref[0, :, 256 * j : 256 * j + 256] = mm(gd_ref[...], ow_ref[j]).astype(bf16)
 
 
 def mix(ret, gact, o):
@@ -201,8 +199,8 @@
         out_shape=jax.ShapeDtypeStruct((1, TOK, 2048), bf16),
         scratch_shapes=[
             pltpu.VMEM((TOK, 1024), bf16),
-            pltpu.VMEM((4, 1024, 512), bf16),
-            pltpu.SemaphoreType.DMA((4,)),
+            pltpu.VMEM((8, 1024, 256), bf16),
+            pltpu.SemaphoreType.DMA((8,)),
         ],
         compiler_params=pltpu.CompilerParams(vmem_limit_bytes=16 * 1024 * 1024),
         cost_estimate=pl.CostEstimate(flops=2 * 128 * 1024 * 2048, bytes_accessed=6 << 20, transcendentals=0),

time: 135 us -> 135 us (level)
  local copies, waits for them, and re-layouts: 6.36 us -> 0 us
  Pallas kernels: 16.2 us -> 22 us
    unnamed x6 -> x0, local copies, waits for them, and re-layouts: 6.36 us -> none
    pallas_call x1, Pallas kernels: 4.32 us -> 9.27 us  [gate(): pl.pallas_call(gate_kernel, grid=(8,), in_specs=[pl.BlockSpec((1, TOK, 25...]
  transfers between devices with their start and end apart: 2 -> 2, of which waited for: 1 -> 1; matrix products, arithmetic and copies ran while one was open for 0% -> 0% of each run, Pallas kernels for 8% -> 11%
where the time goes in v5:
time: 135 us; the launch traced here: 134 us
  blocking collectives  70.1 us (52%)
  Pallas kernels  22 us (16%)
  waiting for transfers between devices  15 us (11%)
  starting transfers between devices  13.6 us (10%)
  between operations  13.4 us (10%)
    all_to_all x1, blocking collectives, shards(): buf = lax.all_to_all(buf, 'sp', split_axis=0, concat_axis=0, tiled=True)  36.8 us
    all_gather x1, blocking collectives, shards(): joined = lax.all_gather(joined, 'sp', axis=0, tiled=True)  33.3 us
    all_gather x1, waiting for transfers between devices, shards(): w = lax.all_gather(joined.reshape(1, 1024, TOK), 'dp', axis=0, tiled=True)  14.9 us
    all_to_all x1, starting transfers between devices, shards(): ret = lax.all_to_all(heads, 'sp', split_axis=0, concat_axis=0, tiled=True)  13.6 us
    pallas_call x1, Pallas kernels, gate(): pl.pallas_call(gate_kernel, grid=(8,), in_specs=[pl.BlockSpec((1, TOK, 25...  9.27 us
    pallas_call x1, Pallas kernels, attend(): pl.pallas_call(attn_kernel, out_shape=jax.ShapeDtypeStruct((SRC, 64, TOK)...  6.03 us
    pallas_call x1, Pallas kernels, mix(): pl.pallas_call(mix_kernel, in_specs=[pl.BlockSpec(memory_space=pltpu.VMEM...  4.24 us
  transfers between devices with their start and end apart: 2, of which 1 were waited for; matrix products, arithmetic and copies ran while one was open for 0% of the time, Pallas kernels for 11%

profile of v5, /device:TPU:1, one launch (start us, length us, event | category | flops | bytes accessed | tf_op | source)
XLA Modules:
  0.0 134.1 jit_solution(16208901169620444831)
XLA Ops:
  6.5 0.0 all-gather.3.cloned.1.call-start
  6.5 2.5 %shard_map.73 = (bf16[16,200,128]{2,1,0:T(8,128)(2,1)}, bf16[64,128]{1,0:T(8,128)(2,1)}) custom-call(bf16[1,128,1024]{2,1,0:T(8,128)(2,1)} %q_ref.1, bf16[1,128,1024]{2,1,0:T(8,128)(2,1)} %k_ref.1, bf16[1,128,1024]{2,1,0:T(8,128)(2,1)} %v_ref.1, bf16[1,16,128]{2,1,0:T(8,128)(2,1)} %bitcast.3, bf16[64,64]{1,0:T(8,128)(2,1)} %gw_ref.1, bf16[64,64]{1,0:T(8,128)(2,1)} %ow_ref.1), custom_call_target="tpu_custom_call" | custom-call | tf_op jit(solution)/shard_map/pallas_call | solution.py:39
  9.0 33.3 %all_gather.6 = bf16[1024,128]{1,0:T(8,128)(2,1)} all-gather(bf16[64,128]{1,0:T(8,128)(2,1)} %get-tuple-element.12), channel_id=1, replica_groups=mesh['sp'=16,'dp'=32] {'sp'}, dimensions={0}, use_global_device_ids=true | all-gather | bytes 278528 | tf_op jit(solution)/shard_map/all_gather | solution.py:212
  42.3 0.0 all-gather.3.cloned.1.call-update
  42.4 36.8 %all_to_all.10.buf_ref = bf16[16,200,128]{2,1,0:T(8,128)(2,1)S(1)} all-to-all(bf16[16,200,128]{2,1,0:T(8,128)(2,1)} %get-tuple-element.13), channel_id=1, replica_groups=mesh['sp'=16,'dp'=32] {'sp'}, dimensions={0} | all-to-all | bytes 1638400 | tf_op jit(solution)/shard_map/all_to_all | solution.py:215
  79.1 6.0 %shard_map.74 = bf16[16,64,128]{2,1,0:T(8,128)(2,1)} custom-call(bf16[16,200,128]{2,1,0:T(8,128)(2,1)S(1)} %all_to_all.10.buf_ref), custom_call_target="tpu_custom_call" | custom-call | tf_op jit(solution)/shard_map/pallas_call | solution.py:124
  85.2 13.6 %all-to-all-start.1 = ((bf16[16,64,128]{2,1,0:T(8,128)(2,1)}), bf16[16,64,128]{2,1,0:T(8,128)(2,1)S(1)}, u32[]{:S(2)}, u32[]{:S(2)}) async-start(bf16[16,64,128]{2,1,0:T(8,128)(2,1)} %shard_map.74), calls=%async_computation.1 | async-start | bytes 524288 | tf_op jit(solution)/shard_map/all_to_all | solution.py:217
  98.8 14.9 %all-gather.3.cloned.1.call-done = bf16[32768,128]{1,0:T(8,128)(2,1)} async-done(((bf16[1024,128]{1,0:T(8,128)(2,1)}), bf16[32768,128]{1,0:T(8,128)(2,1)}) %all-gather.3.cloned.1.call-update) | async-done | bytes 8388624 | tf_op jit(solution)/shard_map/all_gather | solution.py:214
  113.8 9.3 %shard_map.75 = (f32[128,1024]{1,0:T(8,128)S(1)}, bf16[8,1024,256]{2,1,0:T(8,128)(2,1)}) custom-call(bf16[1,128,2048]{2,1,0:T(8,128)(2,1)} %h_ref.1, bf16[32,1024,128]{2,1,0:T(8,128)(2,1)} %bitcast.2), custom_call_target="tpu_custom_call" | custom-call | flops 536870912 | bytes 12582912 | tf_op jit(solution)/shard_map/pallas_call | solution.py:158
  123.0 0.0 all-to-all-done.1.r_ref
  123.0 4.2 %shard_map.76 = bf16[1,128,2048]{2,1,0:T(8,128)(2,1)} custom-call(bf16[16,64,128]{2,1,0:T(8,128)(2,1)S(1)} %all-to-all-done.1.r_ref, f32[128,1024]{1,0:T(8,128)S(1)} %get-tuple-element.15.g_ref, bf16[8,1024,256]{2,1,0:T(8,128)(2,1)} %get-tuple-element.16.o_ref), custom_call_target="tpu_custom_call" | custom-call | flops 536870912 | bytes 6291456 | tf_op jit(solution)/shard_map/pallas_call | solution.py:192
Async XLA Ops:
  6.5 107.2 %all-gather.3.cloned.1.call-start = ((), (), s32[]{:S(2)}) async-start(), calls=%async_computation.2 | async-start | bytes 8650752 | tf_op jit(solution)/shard_map/all_gather | solution.py:214
  85.2 37.9 %all-to-all-start.1 = ((bf16[16,64,128]{2,1,0:T(8,128)(2,1)}), bf16[16,64,128]{2,1,0:T(8,128)(2,1)S(1)}, u32[]{:S(2)}, u32[]{:S(2)}) async-start(bf16[16,64,128]{2,1,0:T(8,128)(2,1)} %shard_map.74), calls=%async_computation.1 | async-start | bytes 524288 | tf_op jit(solution)/shard_map/all_to_all | solution.py:217
Sparse Core Ops, SparseCore 0:
  42.5 71.2 all-gather.2

commit v6 on v2

--- a/solution.py
+++ b/solution.py
@@ -19,13 +19,15 @@
     return lax.dot_general(a, b, (((ca,), (cb,)), ((), ())), preferred_element_type=f32)
 
 
-def pack_kernel(q_ref, k_ref, v_ref, o_ref, out_ref):
+def pack_kernel(q_ref, k_ref, v_ref, o_ref, gw_ref, ow_ref, out_ref, joined_ref):
     row = lax.broadcasted_iota(jnp.int32, (TOK, TOK), 0)
     col = lax.broadcasted_iota(jnp.int32, (TOK, TOK), 1)
     perm = jnp.where(col == GRP * (row % 32) + row // 32, 1.0, 0.0).astype(bf16)
     keys = mm(perm, k_ref[0]).astype(bf16)
     vals = mm(perm, v_ref[0]).astype(bf16)
-    offs = mm(o_ref[0], perm, 0, 1).astype(bf16)
+    offs = mm(o_ref[0], perm, 1, 1).astype(bf16)
+    eye = jnp.where(row[0:HD, 0:HD] == col[0:HD, 0:HD], 1.0, 0.0).astype(bf16)
+    joined_ref[...] = jnp.concatenate([mm(gw_ref[...], eye, 0, 0).astype(bf16), ow_ref[...]], axis=1)
     for h in range(SRC):
         s = slice(HD * h, HD * h + HD)
         out_ref[h, 0:TOK, :] = jnp.concatenate([q_ref[0, :, s], keys[:, s]], axis=1)
@@ -33,11 +35,11 @@
         out_ref[h, 192:200, :] = jnp.broadcast_to(offs[h : h + 1, :], (8, TOK))
 
 
-def pack(q, k, v, o):
+def pack(q, k, v, o, gw, ow):
     return pl.pallas_call(
         pack_kernel,
-        out_shape=jax.ShapeDtypeStruct((SRC, ROWS, TOK), bf16),
-    )(q, k, v, o)
+        out_shape=[jax.ShapeDtypeStruct((SRC, ROWS, TOK), bf16), jax.ShapeDtypeStruct((HD, TOK), bf16)],
+    )(q, k, v, o.transpose(0, 2, 1), gw, ow)
 
 
 def attn_kernel(buf_ref, out_ref, qq, kk, vv, of):
@@ -66,7 +68,7 @@
     tc = lax.broadcasted_iota(jnp.int32, (256, 256), 1)
     tri = jnp.where((tc >= TOK) | (tr > tc), -1.0, 0.0).astype(bf16)
 
-    R = 256
+    R = 512
 
     def block(qt, b, qrow, carry, acc, diag):
         ks = b * 512
@@ -219,9 +221,7 @@
 
 
 def shards(queries, key_rows, value_rows, break_offset, hidden_in, gate_weight, out_weight):
-    buf = pack(queries, key_rows, value_rows, break_offset)
-    joined = jnp.concatenate([gate_weight.T, out_weight], axis=1)
-    buf, joined = lax.optimization_barrier((buf, joined))
+    buf, joined = pack(queries, key_rows, value_rows, break_offset, gate_weight, out_weight)
     joined = lax.all_gather(joined, "sp", axis=0, tiled=True)
     buf, joined = lax.optimization_barrier((buf, joined))
     buf = lax.all_to_all(buf, "sp", split_axis=0, concat_axis=0, tiled=True)

time: 153 us -> 148 us (0.967)
  Pallas kernels: 19.6 us -> 17.2 us
  local copies, waits for them, and re-layouts: 3.51 us -> 1.31 us
    pallas_call x1, Pallas kernels: 8.52 us -> 6.04 us  [attend(): pl.pallas_call(attn_kernel, out_shape=jax.ShapeDtypeStruct((SRC, 64, TOK)...]
    unnamed x6 -> x4, local copies, waits for them, and re-layouts: 2.21 us -> 0.01 us
  transfers between devices with their start and end apart: 12 -> 12, of which waited for: 3 -> 3; matrix products, arithmetic and copies ran while one was open for 2% -> 2% of each run, Pallas kernels for 7% -> 6%
where the time goes in v6:
time: 148 us; the launch traced here: 147 us
  starting transfers between devices  51.6 us (35%)
  blocking collectives  39.5 us (27%)
  waiting for transfers between devices  35.6 us (24%)
  Pallas kernels  17.2 us (12%)
  other arithmetic  1.99 us (1%)
    all_gather x1, blocking collectives, shards(): joined = lax.all_gather(joined, 'sp', axis=0, tiled=True)  39.5 us
    all_to_all x1, waiting for transfers between devices, shards(): ret = lax.all_to_all(heads, 'sp', split_axis=0, concat_axis=0, tiled=True)  15.9 us
    ppermute x2, waiting for transfers between devices, ring(): back3 = lax.ppermute(b, 'dp', moves(phase, -1))  14.1 us
    all_to_all x1, starting transfers between devices, shards(): ret = lax.all_to_all(heads, 'sp', split_axis=0, concat_axis=0, tiled=True)  12 us
    ppermute x2, starting transfers between devices, ring(): top = lax.ppermute(b[..., :64, :], 'dp', moves(phase, 2))  9.34 us
    ppermute x2, starting transfers between devices, ring(): back3 = lax.ppermute(b, 'dp', moves(phase, -1))  7.78 us
    all_to_all x1, starting transfers between devices, shards(): buf = lax.all_to_all(buf, 'sp', split_axis=0, concat_axis=0, tiled=True)  6.56 us
    ppermute x2, starting transfers between devices, ring(): back1 = lax.ppermute(b, 'dp', moves(phase, 1))  6.24 us
  transfers between devices with their start and end apart: 12, of which 3 were waited for; matrix products, arithmetic and copies ran while one was open for 2% of the time, Pallas kernels for 6%

profile of v6, /device:TPU:6, one launch (start us, length us, event | category | flops | bytes accessed | tf_op | source)
XLA Modules:
  0.0 147.5 jit_solution(3998606706529233417)
XLA Ops:
  0.0 2.4 %shard_map.73 = (bf16[16,200,128]{2,1,0:T(8,128)(2,1)}, bf16[64,128]{1,0:T(8,128)(2,1)}) custom-call(bf16[1,128,1024]{2,1,0:T(8,128)(2,1)} %q_ref.1, bf16[1,128,1024]{2,1,0:T(8,128)(2,1)} %k_ref.1, bf16[1,128,1024]{2,1,0:T(8,128)(2,1)} %v_ref.1, bf16[1,16,128]{2,1,0:T(8,128)(2,1)} %bitcast.10, bf16[64,64]{1,0:T(8,128)(2,1)} %gw_ref.1, bf16[64,64]{1,0:T(8,128)(2,1)} %ow_ref.1), custom_call_target="tpu_custom_call" | custom-call | tf_op jit(solution)/shard_map/pallas_call | solution.py:39
  2.4 39.5 %all_gather.3.x_ref = bf16[1024,128]{1,0:T(8,128)(2,1)} all-gather(bf16[64,128]{1,0:T(8,128)(2,1)} %get-tuple-element.10), channel_id=1, replica_groups=mesh['sp'=16,'dp'=32] {'sp'}, dimensions={0}, use_global_device_ids=true | all-gather | bytes 278528 | tf_op jit(solution)/shard_map/all_gather | solution.py:225
  42.0 1.8 %shard_map.75 = bf16[128,1024]{1,0:T(8,128)(2,1)} custom-call(bf16[1024,128]{1,0:T(8,128)(2,1)} %all_gather.3.x_ref), custom_call_target="tpu_custom_call" | custom-call | tf_op jit(solution)/shard_map/pallas_call | solution.py:142
  43.7 0.0 copy-start.1
  43.7 2.9 %collective-permute-start.3 = (bf16[128,1024]{1,0:T(8,128)(2,1)}, bf16[128,1024]{1,0:T(8,128)(2,1)S(1)}, u32[]{:S(2)}, u32[]{:S(2)}) collective-permute-start(bf16[128,1024]{1,0:T(8,128)(2,1)} %shard_map.75), channel_id=1, source_target_pairs={{0,6},{1,25},{2,0},{3,27},{4,2},{5,29},{6,4},{7,31},{8,14},{9,1},{... | collective-permute-start | bytes 786440 | tf_op jit(solution)/shard_map/ppermute | solution.py:217
  46.6 4.3 %collective-permute-start = (bf16[128,1024]{1,0:T(8,128)(2,1)}, bf16[128,1024]{1,0:T(8,128)(2,1)S(1)}, u32[]{:S(2)}, u32[]{:S(2)}) collective-permute-start(bf16[128,1024]{1,0:T(8,128)(2,1)} %shard_map.75), channel_id=1, source_target_pairs={{0,2},{1,9},{2,4},{3,11},{4,6},{5,13},{6,0},{7,15},{8,10},{9,17},{... | collective-permute-start | bytes 786440 | tf_op jit(solution)/shard_map/ppermute | solution.py:216
  50.9 1.0 fusion.3
  51.9 2.1 %collective-permute-start.2 = (bf16[64,1024]{1,0:T(8,128)(2,1)S(1)}, bf16[64,1024]{1,0:T(8,128)(2,1)S(1)}, u32[]{:S(2)}, u32[]{:S(2)}) collective-permute-start(bf16[64,1024]{1,0:T(8,128)(2,1)S(1)} %get-tuple-element.20), channel_id=1, source_target_pairs={{0,4},{1,17},{2,6},{3,19},{4,0},{5,21},{6,2},{7,23},{8,12},{9,25},... | collective-permute-start | bytes 393224 | tf_op jit(solution)/shard_map/ppermute | solution.py:219
  54.0 5.2 %collective-permute-start.1 = (bf16[64,1024]{1,0:T(8,128)(2,1)S(1)}, bf16[64,1024]{1,0:T(8,128)(2,1)S(1)}, u32[]{:S(2)}, u32[]{:S(2)}) collective-permute-start(bf16[64,1024]{1,0:T(8,128)(2,1)S(1)} %get-tuple-element.19), channel_id=1, source_target_pairs={{0,4},{1,17},{2,6},{3,19},{4,0},{5,21},{6,2},{7,23},{8,12},{9,25},... | collective-permute-start | bytes 393224 | tf_op jit(solution)/shard_map/ppermute | solution.py:218
  59.3 6.6 %all-to-all-start = ((bf16[16,200,128]{2,1,0:T(8,128)(2,1)}), bf16[16,200,128]{2,1,0:T(8,128)(2,1)S(1)}, u32[]{:S(2)}, u32[]{:S(2)}) async-start(bf16[16,200,128]{2,1,0:T(8,128)(2,1)} %get-tuple-element.11), calls=%async_computation | async-start | bytes 1638400 | tf_op jit(solution)/shard_map/all_to_all | solution.py:227
  65.8 0.0 collective-permute-done.2
  65.8 0.0 collective-permute-done.1
  65.9 0.0 collective-permute-done.3
  65.9 0.0 collective-permute-done
  65.9 0.0 copy-done.1
  65.9 0.1 pad_maximum_fusion.2
  66.1 4.9 %collective-permute-start.6 = (bf16[4,128,1024]{2,1,0:T(8,128)(2,1)S(1)}, bf16[4,128,1024]{2,1,0:T(8,128)(2,1)S(1)}, u32[]{:S(2)}, u32[]{:S(2)}) collective-permute-start(bf16[4,128,1024]{2,1,0:T(8,128)(2,1)S(1)} %pad_maximum_fusion.2), channel_id=1, source_target_pairs={{0,24},{1,7},{2,26},{3,1},{4,28},{5,3},{6,30},{7,5},{8,0},{9,15},{... | collective-permute-start | bytes 3145736 | tf_op jit(solution)/shard_map/ppermute | solution.py:217
  71.0 1.9 %collective-permute-start.4 = (bf16[4,128,1024]{2,1,0:T(8,128)(2,1)S(1)}, bf16[4,128,1024]{2,1,0:T(8,128)(2,1)S(1)}, u32[]{:S(2)}, u32[]{:S(2)}) collective-permute-start(bf16[4,128,1024]{2,1,0:T(8,128)(2,1)S(1)} %pad_maximum_fusion.2), channel_id=1, source_target_pairs={{0,8},{1,3},{2,10},{3,5},{4,12},{5,7},{6,14},{7,1},{8,16},{9,11},{... | collective-permute-start | bytes 3145736 | tf_op jit(solution)/shard_map/ppermute | solution.py:216
  72.9 0.1 fusion.1
  73.0 4.1 %collective-permute-start.5 = (bf16[4,64,1024]{2,1,0:T(8,128)(2,1)S(1)}, bf16[4,64,1024]{2,1,0:T(8,128)(2,1)S(1)}, u32[]{:S(2)}, u32[]{:S(2)}) collective-permute-start(bf16[4,64,1024]{2,1,0:T(8,128)(2,1)S(1)} %get-tuple-element.16), channel_id=1, source_target_pairs={{0,16},{1,5},{2,18},{3,7},{4,20},{5,1},{6,22},{7,3},{8,24},{9,13},... | collective-permute-start | bytes 1572872 | tf_op jit(solution)/shard_map/ppermute | solution.py:218
  77.1 3.2 %collective-permute-start.8 = (bf16[4,64,1024]{2,1,0:T(8,128)(2,1)S(1)}, bf16[4,64,1024]{2,1,0:T(8,128)(2,1)S(1)}, u32[]{:S(2)}, u32[]{:S(2)}) collective-permute-start(bf16[4,64,1024]{2,1,0:T(8,128)(2,1)S(1)} %get-tuple-element.15), channel_id=1, source_target_pairs={{0,16},{1,5},{2,18},{3,7},{4,20},{5,1},{6,22},{7,3},{8,24},{9,13},... | collective-permute-start | bytes 1572872 | tf_op jit(solution)/shard_map/ppermute | solution.py:219
  80.4 14.1 %collective-permute-done.6 = bf16[4,128,1024]{2,1,0:T(8,128)(2,1)S(1)} collective-permute-done((bf16[4,128,1024]{2,1,0:T(8,128)(2,1)S(1)}, bf16[4,128,1024]{2,1,0:T(8,128)(2,1)S(1)}, u32[]{:S(2)}, u32[]{:S(2)}) %collective-permute-start.6) | collective-permute-done | bytes 1048608 | tf_op jit(solution)/shard_map/ppermute | solution.py:217
  94.5 0.1 fusion.2
  94.6 5.5 %collective-permute-done.4 = bf16[4,128,1024]{2,1,0:T(8,128)(2,1)S(1)} collective-permute-done((bf16[4,128,1024]{2,1,0:T(8,128)(2,1)S(1)}, bf16[4,128,1024]{2,1,0:T(8,128)(2,1)S(1)}, u32[]{:S(2)}, u32[]{:S(2)}) %collective-permute-start.4) | collective-permute-done | bytes 1048608 | tf_op jit(solution)/shard_map/ppermute | solution.py:216
  100.1 0.1 fusion
  100.2 0.0 collective-permute-done.5
  100.2 0.3 pad_maximum_fusion.own_ref
  100.5 1.9 %collective-permute-start.7 = (bf16[16,64,1024]{2,1,0:T(8,128)(2,1)S(1)}, bf16[16,64,1024]{2,1,0:T(8,128)(2,1)}, u32[]{:S(2)}, u32[]{:S(2)}) collective-permute-start(bf16[16,64,1024]{2,1,0:T(8,128)(2,1)S(1)} %pad_maximum_fusion.own_ref), channel_id=1, source_target_pairs={{0,1},{1,0},{2,3},{3,2},{4,5},{5,4},{6,7},{7,6},{8,9},{9,8},{10,11... | collective-permute-start | bytes 6291464 | tf_op jit(solution)/shard_map/ppermute | solution.py:235
  102.4 0.0 collective-permute-done.8
  102.5 0.0 copy-start
  102.5 1.6 %pad_maximum_fusion.1.own_ref = bf16[16,64,1024]{2,1,0:T(8,128)(2,1)} fusion(bf16[4,64,1024]{2,1,0:T(8,128)(2,1)S(1)} %get-tuple-element.17, bf16[4,64,1024]{2,1,0:T(8,128)(2,1)S(1)} %collective-permute-done.8, bf16[4,64,1024]{2,1,0:T(8,128)(2,1)S(1)} %get-tuple-element.13, bf16[4,64,1024]{2,1,0:T(8,128)(2,1)S(1)} %get-tuple-element.15), kind=kLoop, calls=%fused_computation.1 | loop fusion | flops 3145728 | bytes 4194304 | tf_op jit(solution)/shard_map/concatenate | solution.py:233
  104.0 2.4 %collective-permute-start.9 = (bf16[16,64,1024]{2,1,0:T(8,128)(2,1)}, bf16[16,64,1024]{2,1,0:T(8,128)(2,1)}, u32[]{:S(2)}, u32[]{:S(2)}) collective-permute-start(bf16[16,64,1024]{2,1,0:T(8,128)(2,1)} %pad_maximum_fusion.1.own_ref), channel_id=1, source_target_pairs={{0,1},{1,0},{2,3},{3,2},{4,5},{5,4},{6,7},{7,6},{8,9},{9,8},{10,11... | collective-permute-start | bytes 6291464 | tf_op jit(solution)/shard_map/ppermute | solution.py:236
  106.4 0.0 all-to-all-done.buf_ref
  106.5 6.0 %shard_map.74 = bf16[16,64,128]{2,1,0:T(8,128)(2,1)} custom-call(bf16[16,200,128]{2,1,0:T(8,128)(2,1)S(1)} %all-to-all-done.buf_ref), custom_call_target="tpu_custom_call" | custom-call | tf_op jit(solution)/shard_map/pallas_call | solution.py:124
  112.5 12.0 %all-to-all-start.1 = ((bf16[16,64,128]{2,1,0:T(8,128)(2,1)}), bf16[16,64,128]{2,1,0:T(8,128)(2,1)S(1)}, u32[]{:S(2)}, u32[]{:S(2)}) async-start(bf16[16,64,128]{2,1,0:T(8,128)(2,1)} %shard_map.74), calls=%async_computation.1 | async-start | bytes 524288 | tf_op jit(solution)/shard_map/all_to_all | solution.py:239
  124.5 0.0 collective-permute-done.7.sib_ref
  124.5 0.0 copy-done
  124.5 2.4 %shard_map.76.g_ref = f32[128,1024]{1,0:T(8,128)S(1)} custom-call(s32[1]{0:T(128)} %bitcast.pos_ref, bf16[1,128,2048]{2,1,0:T(8,128)(2,1)S(1)} %copy-done, bf16[16,64,1024]{2,1,0:T(8,128)(2,1)S(1)} %pad_maximum_fusion.own_ref, bf16[16,64,1024]{2,1,0:T(8,128)(2,1)} %collective-permute-done.7.sib_ref), custom_call_target="tpu_custom_call" | custom-call | flops 536870912 | bytes 5242880 | tf_op jit(solution)/shard_map/pallas_call | solution.py:184
  126.9 0.0 collective-permute-done.9.sib_ref
  127.0 15.9 %all-to-all-done.1.r_ref = bf16[16,64,128]{2,1,0:T(8,128)(2,1)S(1)} async-done(((bf16[16,64,128]{2,1,0:T(8,128)(2,1)}), bf16[16,64,128]{2,1,0:T(8,128)(2,1)S(1)}, u32[]{:S(2)}, u32[]{:S(2)}) %all-to-all-start.1) | async-done | bytes 262176 | tf_op jit(solution)/shard_map/all_to_all | solution.py:239
  142.9 4.6 %shard_map.77 = bf16[1,128,2048]{2,1,0:T(8,128)(2,1)} custom-call(s32[1]{0:T(128)} %bitcast.pos_ref, bf16[16,64,128]{2,1,0:T(8,128)(2,1)S(1)} %all-to-all-done.1.r_ref, f32[128,1024]{1,0:T(8,128)S(1)} %shard_map.76.g_ref, bf16[16,64,1024]{2,1,0:T(8,128)(2,1)} %pad_maximum_fusion.1.own_ref, bf16[16,64,1024]{2,1,0:T(8,128)(2,1)} %collective-permute-done.9.sib_ref), custom_call_target="tpu_custom_call" | custom-call | flops 536870912 | bytes 6291456 | tf_op jit(solution)/shard_map/pallas_call | solution.py:194
  (1 shorter events, 0.0 us)
Async XLA Ops:
  43.7 22.2 %copy-start.1 = (bf16[128,1024]{1,0:T(8,128)(2,1)S(1)}, bf16[128,1024]{1,0:T(8,128)(2,1)}, u32[]{:S(2)}) copy-start(bf16[128,1024]{1,0:T(8,128)(2,1)} %shard_map.75) | copy-start | bytes 786436
  43.7 22.2 %collective-permute-start.3 = (bf16[128,1024]{1,0:T(8,128)(2,1)}, bf16[128,1024]{1,0:T(8,128)(2,1)S(1)}, u32[]{:S(2)}, u32[]{:S(2)}) collective-permute-start(bf16[128,1024]{1,0:T(8,128)(2,1)} %shard_map.75), channel_id=1, source_target_pairs={{0,6},{1,25},{2,0},{3,27},{4,2},{5,29},{6,4},{7,31},{8,14},{9,1},{... | collective-permute-start | bytes 786440 | tf_op jit(solution)/shard_map/ppermute | solution.py:217
  46.6 19.3 %collective-permute-start = (bf16[128,1024]{1,0:T(8,128)(2,1)}, bf16[128,1024]{1,0:T(8,128)(2,1)S(1)}, u32[]{:S(2)}, u32[]{:S(2)}) collective-permute-start(bf16[128,1024]{1,0:T(8,128)(2,1)} %shard_map.75), channel_id=1, source_target_pairs={{0,2},{1,9},{2,4},{3,11},{4,6},{5,13},{6,0},{7,15},{8,10},{9,17},{... | collective-permute-start | bytes 786440 | tf_op jit(solution)/shard_map/ppermute | solution.py:216
  51.9 13.9 %collective-permute-start.2 = (bf16[64,1024]{1,0:T(8,128)(2,1)S(1)}, bf16[64,1024]{1,0:T(8,128)(2,1)S(1)}, u32[]{:S(2)}, u32[]{:S(2)}) collective-permute-start(bf16[64,1024]{1,0:T(8,128)(2,1)S(1)} %get-tuple-element.20), channel_id=1, source_target_pairs={{0,4},{1,17},{2,6},{3,19},{4,0},{5,21},{6,2},{7,23},{8,12},{9,25},... | collective-permute-start | bytes 393224 | tf_op jit(solution)/shard_map/ppermute | solution.py:219
  54.0 11.8 %collective-permute-start.1 = (bf16[64,1024]{1,0:T(8,128)(2,1)S(1)}, bf16[64,1024]{1,0:T(8,128)(2,1)S(1)}, u32[]{:S(2)}, u32[]{:S(2)}) collective-permute-start(bf16[64,1024]{1,0:T(8,128)(2,1)S(1)} %get-tuple-element.19), channel_id=1, source_target_pairs={{0,4},{1,17},{2,6},{3,19},{4,0},{5,21},{6,2},{7,23},{8,12},{9,25},... | collective-permute-start | bytes 393224 | tf_op jit(solution)/shard_map/ppermute | solution.py:218
  59.3 47.2 %all-to-all-start = ((bf16[16,200,128]{2,1,0:T(8,128)(2,1)}), bf16[16,200,128]{2,1,0:T(8,128)(2,1)S(1)}, u32[]{:S(2)}, u32[]{:S(2)}) async-start(bf16[16,200,128]{2,1,0:T(8,128)(2,1)} %get-tuple-element.11), calls=%async_computation | async-start | bytes 1638400 | tf_op jit(solution)/shard_map/all_to_all | solution.py:227
  66.1 28.5 %collective-permute-start.6 = (bf16[4,128,1024]{2,1,0:T(8,128)(2,1)S(1)}, bf16[4,128,1024]{2,1,0:T(8,128)(2,1)S(1)}, u32[]{:S(2)}, u32[]{:S(2)}) collective-permute-start(bf16[4,128,1024]{2,1,0:T(8,128)(2,1)S(1)} %pad_maximum_fusion.2), channel_id=1, source_target_pairs={{0,24},{1,7},{2,26},{3,1},{4,28},{5,3},{6,30},{7,5},{8,0},{9,15},{... | collective-permute-start | bytes 3145736 | tf_op jit(solution)/shard_map/ppermute | solution.py:217
  71.0 29.1 %collective-permute-start.4 = (bf16[4,128,1024]{2,1,0:T(8,128)(2,1)S(1)}, bf16[4,128,1024]{2,1,0:T(8,128)(2,1)S(1)}, u32[]{:S(2)}, u32[]{:S(2)}) collective-permute-start(bf16[4,128,1024]{2,1,0:T(8,128)(2,1)S(1)} %pad_maximum_fusion.2), channel_id=1, source_target_pairs={{0,8},{1,3},{2,10},{3,5},{4,12},{5,7},{6,14},{7,1},{8,16},{9,11},{... | collective-permute-start | bytes 3145736 | tf_op jit(solution)/shard_map/ppermute | solution.py:216
  73.0 27.2 %collective-permute-start.5 = (bf16[4,64,1024]{2,1,0:T(8,128)(2,1)S(1)}, bf16[4,64,1024]{2,1,0:T(8,128)(2,1)S(1)}, u32[]{:S(2)}, u32[]{:S(2)}) collective-permute-start(bf16[4,64,1024]{2,1,0:T(8,128)(2,1)S(1)} %get-tuple-element.16), channel_id=1, source_target_pairs={{0,16},{1,5},{2,18},{3,7},{4,20},{5,1},{6,22},{7,3},{8,24},{9,13},... | collective-permute-start | bytes 1572872 | tf_op jit(solution)/shard_map/ppermute | solution.py:218
  77.1 25.3 %collective-permute-start.8 = (bf16[4,64,1024]{2,1,0:T(8,128)(2,1)S(1)}, bf16[4,64,1024]{2,1,0:T(8,128)(2,1)S(1)}, u32[]{:S(2)}, u32[]{:S(2)}) collective-permute-start(bf16[4,64,1024]{2,1,0:T(8,128)(2,1)S(1)} %get-tuple-element.15), channel_id=1, source_target_pairs={{0,16},{1,5},{2,18},{3,7},{4,20},{5,1},{6,22},{7,3},{8,24},{9,13},... | collective-permute-start | bytes 1572872 | tf_op jit(solution)/shard_map/ppermute | solution.py:219
  100.5 24.0 %collective-permute-start.7 = (bf16[16,64,1024]{2,1,0:T(8,128)(2,1)S(1)}, bf16[16,64,1024]{2,1,0:T(8,128)(2,1)}, u32[]{:S(2)}, u32[]{:S(2)}) collective-permute-start(bf16[16,64,1024]{2,1,0:T(8,128)(2,1)S(1)} %pad_maximum_fusion.own_ref), channel_id=1, source_target_pairs={{0,1},{1,0},{2,3},{3,2},{4,5},{5,4},{6,7},{7,6},{8,9},{9,8},{10,11... | collective-permute-start | bytes 6291464 | tf_op jit(solution)/shard_map/ppermute | solution.py:235
  102.5 22.1 %copy-start = (bf16[1,128,2048]{2,1,0:T(8,128)(2,1)S(1)}, bf16[1,128,2048]{2,1,0:T(8,128)(2,1)}, u32[]{:S(2)}) copy-start(bf16[1,128,2048]{2,1,0:T(8,128)(2,1)} %h_ref.1) | copy-start | bytes 1572868
  104.0 22.9 %collective-permute-start.9 = (bf16[16,64,1024]{2,1,0:T(8,128)(2,1)}, bf16[16,64,1024]{2,1,0:T(8,128)(2,1)}, u32[]{:S(2)}, u32[]{:S(2)}) collective-permute-start(bf16[16,64,1024]{2,1,0:T(8,128)(2,1)} %pad_maximum_fusion.1.own_ref), channel_id=1, source_target_pairs={{0,1},{1,0},{2,3},{3,2},{4,5},{5,4},{6,7},{7,6},{8,9},{9,8},{10,11... | collective-permute-start | bytes 6291464 | tf_op jit(solution)/shard_map/ppermute | solution.py:236
  112.5 30.4 %all-to-all-start.1 = ((bf16[16,64,128]{2,1,0:T(8,128)(2,1)}), bf16[16,64,128]{2,1,0:T(8,128)(2,1)S(1)}, u32[]{:S(2)}, u32[]{:S(2)}) async-start(bf16[16,64,128]{2,1,0:T(8,128)(2,1)} %shard_map.74), calls=%async_computation.1 | async-start | bytes 524288 | tf_op jit(solution)/shard_map/all_to_all | solution.py:239

commit v7 on v6

--- a/solution.py
+++ b/solution.py
@@ -142,27 +142,35 @@
     return pl.pallas_call(turn_kernel, out_shape=jax.ShapeDtypeStruct((128, 1024), bf16))(x)
 
 
-def two_chips(pos_ref, own_ref, sib_ref, j):
+def fetch(pos_ref, own_ref, sib_ref, w_ref, sems, half):
     p = pos_ref[0]
-    south, x, y = (p & 1) == 0, (p >> 1) & 3, p >> 3
-    rows = []
-    for chip in (2 * j, 2 * j + 1):
+    core, x, y = p & 1, (p >> 1) & 3, p >> 3
+    copies = []
+    for chip in range(16):
         dy, dx = (y - chip // 4) & 3, (x - chip % 4) & 3
         first, second = 4 * dy + dx, 4 * dx + dy
-        a = own_ref[jnp.where(south, first, second)]
-        b = sib_ref[jnp.where(south, second, first)]
-        rows += [jnp.where(south, a, b), jnp.where(south, b, a)]
-    return jnp.concatenate(rows, axis=0)
-
-
-def gate_kernel(pos_ref, h_ref, own_ref, sib_ref, out_ref):
+        mine = first + core * (second - first)
+        other = second + core * (first - second)
+        for k, (ref, slot, c) in enumerate(((own_ref, mine, core), (sib_ref, other, 1 - core))):
+            dst = w_ref.at[chip, c]
+            copies.append(pltpu.make_async_copy(ref.at[slot, half], dst, sems.at[2 * chip + k]))
+    for c in copies:
+        c.start()
+    return copies
+
+
+def gate_kernel(pos_ref, h_ref, own_ref, sib_ref, out_ref, w_ref, sems):
+    copies = fetch(pos_ref, own_ref, sib_ref, w_ref, sems, 0)
     acc = jnp.zeros((TOK, 1024), f32)
     for j in range(8):
-        acc = acc + mm(h_ref[0, :, 256 * j : 256 * j + 256], two_chips(pos_ref, own_ref, sib_ref, j))
+        for c in copies[4 * j : 4 * j + 4]:
+            c.wait()
+        acc = acc + mm(h_ref[0, :, 256 * j : 256 * j + 256], w_ref[2 * j : 2 * j + 2].reshape(256, 1024))
     out_ref[...] = acc / (1.0 + jnp.exp(-acc))
 
 
-def mix_kernel(pos_ref, r_ref, g_ref, own_ref, sib_ref, out_ref, gd_ref):
+def mix_kernel(pos_ref, r_ref, g_ref, own_ref, sib_ref, out_ref, gd_ref, w_ref, sems):
+    copies = fetch(pos_ref, own_ref, sib_ref, w_ref, sems, 1)
     for h in range(0, SRC, 2):
         a, b = r_ref[h], r_ref[h + 1]
         top = jnp.concatenate([a[:, 0:HD], b[:, 0:HD]], axis=1)
@@ -171,34 +179,41 @@
         s = slice(HD * h, HD * h + 2 * HD)
         gd_ref[:, s] = (n * g_ref[:, s]).astype(bf16)
     for j in range(8):
-        w = two_chips(pos_ref, own_ref, sib_ref, j)
+        for c in copies[4 * j : 4 * j + 4]:
+            c.wait()
+        w = w_ref[2 * j : 2 * j + 2].reshape(256, 1024)
         out_ref[0, :, 256 * j : 256 * j + 256] = mm(gd_ref[...], w, 1, 1).astype(bf16)
 
 
-def whole(n, smem=1):
-    spec = [pl.BlockSpec(memory_space=pltpu.SMEM)] * smem
-    return spec + [pl.BlockSpec(memory_space=pltpu.VMEM)] * n
-
-
-def gate(tab, hidden, own, sib):
+def specs(n):
+    vmem = [pl.BlockSpec(memory_space=pltpu.VMEM)] * n
+    return [pl.BlockSpec(memory_space=pltpu.SMEM)] + vmem + [pl.BlockSpec(memory_space=pltpu.HBM)] * 2
+
+
+def gate(pos, hidden, own, sib):
     return pl.pallas_call(
         gate_kernel,
-        in_specs=whole(3),
+        in_specs=specs(1),
         out_shape=jax.ShapeDtypeStruct((TOK, 1024), f32),
-        compiler_params=pltpu.CompilerParams(vmem_limit_bytes=40 * 1024 * 1024),
+        scratch_shapes=[pltpu.VMEM((16, 2, 64, 1024), bf16), pltpu.SemaphoreType.DMA((32,))],
+        compiler_params=pltpu.CompilerParams(vmem_limit_bytes=24 * 1024 * 1024),
         cost_estimate=pl.CostEstimate(flops=2 * 128 * 1024 * 2048, bytes_accessed=5 << 20, transcendentals=1 << 17),
-    )(tab, hidden, own, sib)
-
-
-def mix(tab, ret, gact, own, sib):
+    )(pos, hidden, own, sib)
+
+
+def mix(pos, ret, gact, own, sib):
     return pl.pallas_call(
         mix_kernel,
-        in_specs=whole(4),
+        in_specs=specs(2),
         out_shape=jax.ShapeDtypeStruct((1, TOK, 2048), bf16),
-        scratch_shapes=[pltpu.VMEM((TOK, 1024), bf16)],
-        compiler_params=pltpu.CompilerParams(vmem_limit_bytes=40 * 1024 * 1024),
+        scratch_shapes=[
+            pltpu.VMEM((TOK, 1024), bf16),
+            pltpu.VMEM((16, 2, 64, 1024), bf16),
+            pltpu.SemaphoreType.DMA((32,)),
+        ],
+        compiler_params=pltpu.CompilerParams(vmem_limit_bytes=24 * 1024 * 1024),
         cost_estimate=pl.CostEstimate(flops=2 * 128 * 1024 * 2048, bytes_accessed=6 << 20, transcendentals=0),
-    )(tab, ret, gact, own, sib)
+    )(pos, ret, gact, own, sib)
 
 
 def moves(phase, step):
@@ -229,16 +244,16 @@
     back1, back3, top, bot = ring(b, 1)
     b = jnp.stack([b, back1, jnp.concatenate([top, bot], axis=0), back3])
     back1, back3, top, bot = ring(b, 2)
-    own_g = jnp.concatenate([b[:, :64], back1[:, :64], top, back3[:, :64]], axis=0)
-    own_o = jnp.concatenate([b[:, 64:], back1[:, 64:], bot, back3[:, 64:]], axis=0)
-    swap = [(p, p ^ 1) for p in range(32)]
-    sib_g = lax.ppermute(own_g, "dp", swap)
-    sib_o = lax.ppermute(own_o, "dp", swap)
+    own = jnp.stack([b, back1, jnp.concatenate([top, bot], axis=1), back3])
+    sib = lax.ppermute(own, "dp", [(p, p ^ 1) for p in range(32)])
+    own, sib = (
+        pltpu.with_memory_space_constraint(w.reshape(16, 2, 64, 1024), pltpu.HBM) for w in (own, sib)
+    )
     pos = lax.axis_index("dp").astype(jnp.int32).reshape(1)
     heads = attend(buf)
     ret = lax.all_to_all(heads, "sp", split_axis=0, concat_axis=0, tiled=True)
-    gact = gate(pos, hidden_in, own_g, sib_g)
-    return mix(pos, ret, gact, own_o, sib_o)
+    gact = gate(pos, hidden_in, own, sib)
+    return mix(pos, ret, gact, own, sib)
 
 
 def solution(mesh):

time: 148 us -> 189 us (1.28)
  the two profiles are of different devices: /device:TPU:6 before, /device:TPU:10 now
where the time goes in v7:
time: 189 us; the launch traced here: 188 us
  blocking collectives  88.8 us (47%)
  waiting for transfers between devices  41.2 us (22%)
  starting transfers between devices  34.8 us (18%)
  Pallas kernels  18.8 us (10%)
  other arithmetic  3.47 us (2%)
    all_to_all x1, blocking collectives, shards(): buf = lax.all_to_all(buf, 'sp', split_axis=0, concat_axis=0, tiled=True)  49.3 us
    all_gather x1, blocking collectives, shards(): joined = lax.all_gather(joined, 'sp', axis=0, tiled=True)  39.5 us
    all_to_all x1, waiting for transfers between devices, shards(): ret = lax.all_to_all(heads, 'sp', split_axis=0, concat_axis=0, tiled=True)  15.5 us
    ppermute x2, waiting for transfers between devices, ring(): top = lax.ppermute(b[..., :64, :], 'dp', moves(phase, 2))  14.8 us
    ppermute x2, waiting for transfers between devices, ring(): bot = lax.ppermute(b[..., 64:, :], 'dp', moves(phase, -2))  10.9 us
    ppermute x2, starting transfers between devices, ring(): top = lax.ppermute(b[..., :64, :], 'dp', moves(phase, 2))  10 us
    ppermute x2, starting transfers between devices, ring(): back1 = lax.ppermute(b, 'dp', moves(phase, 1))  8.11 us
    pallas_call x1, Pallas kernels, attend(): pl.pallas_call(attn_kernel, out_shape=jax.ShapeDtypeStruct((SRC, 64, TOK)...  6.03 us
  transfers between devices with their start and end apart: 10, of which 5 were waited for; matrix products, arithmetic and copies ran while one was open for 1% of the time, Pallas kernels for 5%

profile of v7, /device:TPU:10, one launch (start us, length us, event | category | flops | bytes accessed | tf_op | source)
XLA Modules:
  0.0 188.4 jit_solution(14901818785865035964)
XLA Ops:
  0.0 2.5 %shard_map.73 = (bf16[16,200,128]{2,1,0:T(8,128)(2,1)}, bf16[64,128]{1,0:T(8,128)(2,1)}) custom-call(bf16[1,128,1024]{2,1,0:T(8,128)(2,1)} %q_ref.1, bf16[1,128,1024]{2,1,0:T(8,128)(2,1)} %k_ref.1, bf16[1,128,1024]{2,1,0:T(8,128)(2,1)} %v_ref.1, bf16[1,16,128]{2,1,0:T(8,128)(2,1)} %bitcast.20, bf16[64,64]{1,0:T(8,128)(2,1)} %gw_ref.1, bf16[64,64]{1,0:T(8,128)(2,1)} %ow_ref.1), custom_call_target="tpu_custom_call" | custom-call | tf_op jit(solution)/shard_map/pallas_call | solution.py:39
  2.5 39.5 %all_gather.3.x_ref = bf16[1024,128]{1,0:T(8,128)(2,1)} all-gather(bf16[64,128]{1,0:T(8,128)(2,1)} %get-tuple-element.10), channel_id=1, replica_groups=mesh['sp'=16,'dp'=32] {'sp'}, dimensions={0}, use_global_device_ids=true | all-gather | bytes 278528 | tf_op jit(solution)/shard_map/all_gather | solution.py:240
  42.0 1.8 shard_map.75
  43.8 2.4 %collective-permute-start.3 = (bf16[128,1024]{1,0:T(8,128)(2,1)}, bf16[128,1024]{1,0:T(8,128)(2,1)S(1)}, u32[]{:S(2)}, u32[]{:S(2)}) collective-permute-start(bf16[128,1024]{1,0:T(8,128)(2,1)} %shard_map.75), channel_id=1, source_target_pairs={{0,6},{1,25},{2,0},{3,27},{4,2},{5,29},{6,4},{7,31},{8,14},{9,1},{... | collective-permute-start | bytes 786440 | tf_op jit(solution)/shard_map/ppermute | solution.py:232
  46.2 3.4 %collective-permute-start = (bf16[128,1024]{1,0:T(8,128)(2,1)}, bf16[128,1024]{1,0:T(8,128)(2,1)S(1)}, u32[]{:S(2)}, u32[]{:S(2)}) collective-permute-start(bf16[128,1024]{1,0:T(8,128)(2,1)} %shard_map.75), channel_id=1, source_target_pairs={{0,2},{1,9},{2,4},{3,11},{4,6},{5,13},{6,0},{7,15},{8,10},{9,17},{... | collective-permute-start | bytes 786440 | tf_op jit(solution)/shard_map/ppermute | solution.py:231
  49.6 1.0 fusion.2
  50.6 5.2 %collective-permute-start.1 = (bf16[64,1024]{1,0:T(8,128)(2,1)S(1)}, bf16[64,1024]{1,0:T(8,128)(2,1)S(1)}, u32[]{:S(2)}, u32[]{:S(2)}) collective-permute-start(bf16[64,1024]{1,0:T(8,128)(2,1)S(1)} %get-tuple-element.17), channel_id=1, source_target_pairs={{0,4},{1,17},{2,6},{3,19},{4,0},{5,21},{6,2},{7,23},{8,12},{9,25},... | collective-permute-start | bytes 393224 | tf_op jit(solution)/shard_map/ppermute | solution.py:233
  55.9 2.1 %collective-permute-start.2 = (bf16[64,1024]{1,0:T(8,128)(2,1)S(1)}, bf16[64,1024]{1,0:T(8,128)(2,1)S(1)}, u32[]{:S(2)}, u32[]{:S(2)}) collective-permute-start(bf16[64,1024]{1,0:T(8,128)(2,1)S(1)} %get-tuple-element.18), channel_id=1, source_target_pairs={{0,4},{1,17},{2,6},{3,19},{4,0},{5,21},{6,2},{7,23},{8,12},{9,25},... | collective-permute-start | bytes 393224 | tf_op jit(solution)/shard_map/ppermute | solution.py:234
  58.0 1.0 collective-permute-done.1
  59.0 5.3 %collective-permute-done.2 = bf16[64,1024]{1,0:T(8,128)(2,1)S(1)} collective-permute-done((bf16[64,1024]{1,0:T(8,128)(2,1)S(1)}, bf16[64,1024]{1,0:T(8,128)(2,1)S(1)}, u32[]{:S(2)}, u32[]{:S(2)}) %collective-permute-start.2) | collective-permute-done | bytes 131104 | tf_op jit(solution)/shard_map/ppermute | solution.py:234
  64.3 0.0 collective-permute-done.3
  64.3 0.0 collective-permute-done
  64.3 1.1 fusion
  65.4 4.7 %collective-permute-start.4 = (bf16[4,128,1024]{2,1,0:T(8,128)(2,1)S(1)}, bf16[4,128,1024]{2,1,0:T(8,128)(2,1)S(1)}, u32[]{:S(2)}, u32[]{:S(2)}) collective-permute-start(bf16[4,128,1024]{2,1,0:T(8,128)(2,1)S(1)} %get-tuple-element.14), channel_id=1, source_target_pairs={{0,8},{1,3},{2,10},{3,5},{4,12},{5,7},{6,14},{7,1},{8,16},{9,11},{... | collective-permute-start | bytes 3145736 | tf_op jit(solution)/shard_map/ppermute | solution.py:231
  70.2 1.9 %collective-permute-start.7 = (bf16[4,128,1024]{2,1,0:T(8,128)(2,1)S(1)}, bf16[4,128,1024]{2,1,0:T(8,128)(2,1)S(1)}, u32[]{:S(2)}, u32[]{:S(2)}) collective-permute-start(bf16[4,128,1024]{2,1,0:T(8,128)(2,1)S(1)} %get-tuple-element.14), channel_id=1, source_target_pairs={{0,24},{1,7},{2,26},{3,1},{4,28},{5,3},{6,30},{7,5},{8,0},{9,15},{... | collective-permute-start | bytes 3145736 | tf_op jit(solution)/shard_map/ppermute | solution.py:232
  72.1 0.1 fusion.1
  72.2 4.8 %collective-permute-start.5 = (bf16[4,64,1024]{2,1,0:T(8,128)(2,1)S(1)}, bf16[4,64,1024]{2,1,0:T(8,128)(2,1)S(1)}, u32[]{:S(2)}, u32[]{:S(2)}) collective-permute-start(bf16[4,64,1024]{2,1,0:T(8,128)(2,1)S(1)} %get-tuple-element.15), channel_id=1, source_target_pairs={{0,16},{1,5},{2,18},{3,7},{4,20},{5,1},{6,22},{7,3},{8,24},{9,13},... | collective-permute-start | bytes 1572872 | tf_op jit(solution)/shard_map/ppermute | solution.py:233
  77.0 2.6 %collective-permute-start.6 = (bf16[4,64,1024]{2,1,0:T(8,128)(2,1)S(1)}, bf16[4,64,1024]{2,1,0:T(8,128)(2,1)S(1)}, u32[]{:S(2)}, u32[]{:S(2)}) collective-permute-start(bf16[4,64,1024]{2,1,0:T(8,128)(2,1)S(1)} %get-tuple-element.16), channel_id=1, source_target_pairs={{0,16},{1,5},{2,18},{3,7},{4,20},{5,1},{6,22},{7,3},{8,24},{9,13},... | collective-permute-start | bytes 1572872 | tf_op jit(solution)/shard_map/ppermute | solution.py:234
  79.5 13.8 %collective-permute-done.5 = bf16[4,64,1024]{2,1,0:T(8,128)(2,1)S(1)} collective-permute-done((bf16[4,64,1024]{2,1,0:T(8,128)(2,1)S(1)}, bf16[4,64,1024]{2,1,0:T(8,128)(2,1)S(1)}, u32[]{:S(2)}, u32[]{:S(2)}) %collective-permute-start.5) | collective-permute-done | bytes 524320 | tf_op jit(solution)/shard_map/ppermute | solution.py:233
  93.3 5.6 %collective-permute-done.6 = bf16[4,64,1024]{2,1,0:T(8,128)(2,1)S(1)} collective-permute-done((bf16[4,64,1024]{2,1,0:T(8,128)(2,1)S(1)}, bf16[4,64,1024]{2,1,0:T(8,128)(2,1)S(1)}, u32[]{:S(2)}, u32[]{:S(2)}) %collective-permute-start.6) | collective-permute-done | bytes 524320 | tf_op jit(solution)/shard_map/ppermute | solution.py:234
  99.0 0.1 maximum_bitcast_fusion
  99.1 0.0 collective-permute-done.4
  99.1 0.0 collective-permute-done.7
  99.1 0.0 copy-start.1
  99.1 0.0 copy-start
  99.1 2.2 %pad_maximum_fusion = bf16[4,4,128,1024]{3,2,1,0:T(8,128)(2,1)} fusion(bf16[1,4,128,1024]{3,2,1,0:T(8,128)(2,1)S(1)} %bitcast.17, bf16[1,4,128,1024]{3,2,1,0:T(8,128)(2,1)S(1)} %maximum_bitcast_fusion, bf16[1,4,128,1024]{3,2,1,0:T(8,128)(2,1)S(1)} %bitcast.16, bf16[1,4,128,1024]{3,2,1,0:T(8,128)(2,1)S(1)} %get-tuple-element.13), kind=kLoop, calls=%fused_computation | loop fusion | flops 6291456 | bytes 8388608 | tf_op jit(solution)/shard_map/stack | solution.py:247
  101.3 1.9 %collective-permute-start.8 = (bf16[4,4,128,1024]{3,2,1,0:T(8,128)(2,1)}, bf16[4,4,128,1024]{3,2,1,0:T(8,128)(2,1)}, u32[]{:S(2)}, u32[]{:S(2)}) collective-permute-start(bf16[4,4,128,1024]{3,2,1,0:T(8,128)(2,1)} %pad_maximum_fusion), channel_id=1, source_target_pairs={{0,1},{1,0},{2,3},{3,2},{4,5},{5,4},{6,7},{7,6},{8,9},{9,8},{10,11... | collective-permute-start | bytes 12582920 | tf_op jit(solution)/shard_map/ppermute | solution.py:248
  103.3 0.0 copy-done.1
  103.3 49.3 %all_to_all.10.buf_ref = bf16[16,200,128]{2,1,0:T(8,128)(2,1)S(1)} all-to-all(bf16[16,200,128]{2,1,0:T(8,128)(2,1)S(1)} %copy-done.1), channel_id=1, replica_groups=mesh['sp'=16,'dp'=32] {'sp'}, dimensions={0} | all-to-all | bytes 1638400 | tf_op jit(solution)/shard_map/all_to_all | solution.py:242
  152.6 6.0 %shard_map.74 = bf16[16,64,128]{2,1,0:T(8,128)(2,1)} custom-call(bf16[16,200,128]{2,1,0:T(8,128)(2,1)S(1)} %all_to_all.10.buf_ref), custom_call_target="tpu_custom_call" | custom-call | tf_op jit(solution)/shard_map/pallas_call | solution.py:124
  158.6 5.7 %all-to-all-start.1 = ((bf16[16,64,128]{2,1,0:T(8,128)(2,1)}), bf16[16,64,128]{2,1,0:T(8,128)(2,1)S(1)}, u32[]{:S(2)}, u32[]{:S(2)}) async-start(bf16[16,64,128]{2,1,0:T(8,128)(2,1)} %shard_map.74), calls=%async_computation.1 | async-start | bytes 524288 | tf_op jit(solution)/shard_map/all_to_all | solution.py:254
  164.3 0.0 collective-permute-done.8
  164.4 0.0 copy-done
  164.4 2.8 %shard_map.76.g_ref = f32[128,1024]{1,0:T(8,128)S(1)} custom-call(s32[1]{0:T(128)} %bitcast.pos_ref, bf16[1,128,2048]{2,1,0:T(8,128)(2,1)S(1)} %copy-done, bf16[16,2,64,1024]{3,2,1,0:T(8,128)(2,1)} %bitcast.10.own_ref, bf16[16,2,64,1024]{3,2,1,0:T(8,128)(2,1)} %bitcast.11.sib_ref), custom_call_target="tpu_custom_call" | custom-call | flops 536870912 | bytes 5242880 | tf_op jit(solution)/shard_map/pallas_call | solution.py:194
  167.2 15.5 %all-to-all-done.1.r_ref = bf16[16,64,128]{2,1,0:T(8,128)(2,1)S(1)} async-done(((bf16[16,64,128]{2,1,0:T(8,128)(2,1)}), bf16[16,64,128]{2,1,0:T(8,128)(2,1)S(1)}, u32[]{:S(2)}, u32[]{:S(2)}) %all-to-all-start.1) | async-done | bytes 262176 | tf_op jit(solution)/shard_map/all_to_all | solution.py:254
  182.7 5.7 %shard_map.77 = bf16[1,128,2048]{2,1,0:T(8,128)(2,1)} custom-call(s32[1]{0:T(128)} %bitcast.pos_ref, bf16[16,64,128]{2,1,0:T(8,128)(2,1)S(1)} %all-to-all-done.1.r_ref, f32[128,1024]{1,0:T(8,128)S(1)} %shard_map.76.g_ref, bf16[16,2,64,1024]{3,2,1,0:T(8,128)(2,1)} %bitcast.10.own_ref, bf16[16,2,64,1024]{3,2,1,0:T(8,128)(2,1)} %bitcast.11.sib_ref), custom_call_target="tpu_custom_call" | custom-call | flops 536870912 | bytes 6291456 | tf_op jit(solution)/shard_map/pallas_call | solution.py:205
  (1 shorter events, 0.0 us)
Async XLA Ops:
  43.8 20.5 %collective-permute-start.3 = (bf16[128,1024]{1,0:T(8,128)(2,1)}, bf16[128,1024]{1,0:T(8,128)(2,1)S(1)}, u32[]{:S(2)}, u32[]{:S(2)}) collective-permute-start(bf16[128,1024]{1,0:T(8,128)(2,1)} %shard_map.75), channel_id=1, source_target_pairs={{0,6},{1,25},{2,0},{3,27},{4,2},{5,29},{6,4},{7,31},{8,14},{9,1},{... | collective-permute-start | bytes 786440 | tf_op jit(solution)/shard_map/ppermute | solution.py:232
  46.2 18.1 %collective-permute-start = (bf16[128,1024]{1,0:T(8,128)(2,1)}, bf16[128,1024]{1,0:T(8,128)(2,1)S(1)}, u32[]{:S(2)}, u32[]{:S(2)}) collective-permute-start(bf16[128,1024]{1,0:T(8,128)(2,1)} %shard_map.75), channel_id=1, source_target_pairs={{0,2},{1,9},{2,4},{3,11},{4,6},{5,13},{6,0},{7,15},{8,10},{9,17},{... | collective-permute-start | bytes 786440 | tf_op jit(solution)/shard_map/ppermute | solution.py:231
  50.6 8.4 %collective-permute-start.1 = (bf16[64,1024]{1,0:T(8,128)(2,1)S(1)}, bf16[64,1024]{1,0:T(8,128)(2,1)S(1)}, u32[]{:S(2)}, u32[]{:S(2)}) collective-permute-start(bf16[64,1024]{1,0:T(8,128)(2,1)S(1)} %get-tuple-element.17), channel_id=1, source_target_pairs={{0,4},{1,17},{2,6},{3,19},{4,0},{5,21},{6,2},{7,23},{8,12},{9,25},... | collective-permute-start | bytes 393224 | tf_op jit(solution)/shard_map/ppermute | solution.py:233
  55.9 8.4 %collective-permute-start.2 = (bf16[64,1024]{1,0:T(8,128)(2,1)S(1)}, bf16[64,1024]{1,0:T(8,128)(2,1)S(1)}, u32[]{:S(2)}, u32[]{:S(2)}) collective-permute-start(bf16[64,1024]{1,0:T(8,128)(2,1)S(1)} %get-tuple-element.18), channel_id=1, source_target_pairs={{0,4},{1,17},{2,6},{3,19},{4,0},{5,21},{6,2},{7,23},{8,12},{9,25},... | collective-permute-start | bytes 393224 | tf_op jit(solution)/shard_map/ppermute | solution.py:234
  65.4 33.6 %collective-permute-start.4 = (bf16[4,128,1024]{2,1,0:T(8,128)(2,1)S(1)}, bf16[4,128,1024]{2,1,0:T(8,128)(2,1)S(1)}, u32[]{:S(2)}, u32[]{:S(2)}) collective-permute-start(bf16[4,128,1024]{2,1,0:T(8,128)(2,1)S(1)} %get-tuple-element.14), channel_id=1, source_target_pairs={{0,8},{1,3},{2,10},{3,5},{4,12},{5,7},{6,14},{7,1},{8,16},{9,11},{... | collective-permute-start | bytes 3145736 | tf_op jit(solution)/shard_map/ppermute | solution.py:231
  70.2 28.9 %collective-permute-start.7 = (bf16[4,128,1024]{2,1,0:T(8,128)(2,1)S(1)}, bf16[4,128,1024]{2,1,0:T(8,128)(2,1)S(1)}, u32[]{:S(2)}, u32[]{:S(2)}) collective-permute-start(bf16[4,128,1024]{2,1,0:T(8,128)(2,1)S(1)} %get-tuple-element.14), channel_id=1, source_target_pairs={{0,24},{1,7},{2,26},{3,1},{4,28},{5,3},{6,30},{7,5},{8,0},{9,15},{... | collective-permute-start | bytes 3145736 | tf_op jit(solution)/shard_map/ppermute | solution.py:232
  72.2 21.2 %collective-permute-start.5 = (bf16[4,64,1024]{2,1,0:T(8,128)(2,1)S(1)}, bf16[4,64,1024]{2,1,0:T(8,128)(2,1)S(1)}, u32[]{:S(2)}, u32[]{:S(2)}) collective-permute-start(bf16[4,64,1024]{2,1,0:T(8,128)(2,1)S(1)} %get-tuple-element.15), channel_id=1, source_target_pairs={{0,16},{1,5},{2,18},{3,7},{4,20},{5,1},{6,22},{7,3},{8,24},{9,13},... | collective-permute-start | bytes 1572872 | tf_op jit(solution)/shard_map/ppermute | solution.py:233
  77.0 22.0 %collective-permute-start.6 = (bf16[4,64,1024]{2,1,0:T(8,128)(2,1)S(1)}, bf16[4,64,1024]{2,1,0:T(8,128)(2,1)S(1)}, u32[]{:S(2)}, u32[]{:S(2)}) collective-permute-start(bf16[4,64,1024]{2,1,0:T(8,128)(2,1)S(1)} %get-tuple-element.16), channel_id=1, source_target_pairs={{0,16},{1,5},{2,18},{3,7},{4,20},{5,1},{6,22},{7,3},{8,24},{9,13},... | collective-permute-start | bytes 1572872 | tf_op jit(solution)/shard_map/ppermute | solution.py:234
  99.1 4.2 %copy-start.1 = (bf16[16,200,128]{2,1,0:T(8,128)(2,1)S(1)}, bf16[16,200,128]{2,1,0:T(8,128)(2,1)}, u32[]{:S(2)}) copy-start(bf16[16,200,128]{2,1,0:T(8,128)(2,1)} %get-tuple-element.11) | copy-start | bytes 2457604
  99.1 65.3 %copy-start = (bf16[1,128,2048]{2,1,0:T(8,128)(2,1)S(1)}, bf16[1,128,2048]{2,1,0:T(8,128)(2,1)}, u32[]{:S(2)}) copy-start(bf16[1,128,2048]{2,1,0:T(8,128)(2,1)} %h_ref.1) | copy-start | bytes 1572868
  101.3 63.0 %collective-permute-start.8 = (bf16[4,4,128,1024]{3,2,1,0:T(8,128)(2,1)}, bf16[4,4,128,1024]{3,2,1,0:T(8,128)(2,1)}, u32[]{:S(2)}, u32[]{:S(2)}) collective-permute-start(bf16[4,4,128,1024]{3,2,1,0:T(8,128)(2,1)} %pad_maximum_fusion), channel_id=1, source_target_pairs={{0,1},{1,0},{2,3},{3,2},{4,5},{5,4},{6,7},{7,6},{8,9},{9,8},{10,11... | collective-permute-start | bytes 12582920 | tf_op jit(solution)/shard_map/ppermute | solution.py:248
  158.6 24.2 %all-to-all-start.1 = ((bf16[16,64,128]{2,1,0:T(8,128)(2,1)}), bf16[16,64,128]{2,1,0:T(8,128)(2,1)S(1)}, u32[]{:S(2)}, u32[]{:S(2)}) async-start(bf16[16,64,128]{2,1,0:T(8,128)(2,1)} %shard_map.74), calls=%async_computation.1 | async-start | bytes 524288 | tf_op jit(solution)/shard_map/all_to_all | solution.py:254
